TPU v7x, 32 devices: a whole 2x2x4 slice. The times are simulated.
32 devices in a mesh: ep: 16 (over z, y, x), tp: 2 (over core).
Axes of the slice: x: 2, y: 2, z: 4, core: 2. Of those that a mesh axis runs over, the one named last changes fastest.
Arguments:
- stream: bfloat16 [512, 2048], P('ep'), may hold values from -6 to 6
- mixer_gain: float32 [2048], replicated, may hold values from 0.1 to 1.9
- gate_proj: bfloat16 [2048, 1024], P(None, 'tp'), may hold values from -0.125 to 0.125
- input_proj: bfloat16 [2048, 1024], P(None, 'tp'), may hold values from -0.125 to 0.125
- state_maps: bfloat16 [2, 2048, 256], P(None, None, 'tp'), may hold values from -0.125 to 0.125
- step_proj: bfloat16 [2048, 16], P(None, 'tp'), may hold values from -0.125 to 0.125
- step_bias: float32 [16], P('tp'), may hold values from -3 to 0.5
- decay_rate: float32 [16], P('tp'), may hold values from 0.05 to 4
- input_taps: float32 [4, 1024], P(None, 'tp'), may hold values from -3 to 3
- map_taps: float32 [2, 4, 256], P(None, None, 'tp'), may hold values from -3 to 3
- input_past: bfloat16 [512, 3, 1024], P('ep', None, 'tp'), may hold values from -6 to 6
- map_past: bfloat16 [512, 2, 3, 256], P('ep', None, None, 'tp'), may hold values from -6 to 6
- head_state: float32 [512, 16, 4096], P('ep', 'tp'), may hold values from -1.6 to 1.6
- skip_gain: float32 [16], P('tp'), may hold values from 0 to 2
- inner_gain: float32 [1024], P('tp'), may hold values from 0.1 to 1.9
- mixer_out: bfloat16 [1024, 2048], P('tp'), may hold values from -0.1875 to 0.1875
- channel_gain: float32 [2048], replicated, may hold values from 0.1 to 1.9
- expert_ids: int32 [512, 2], P('ep'), may hold values from 0 to 7, all different within a row; in each aligned block of 32 rows (0 to 31, 32 to 63, ...) at most 12 rows name the same one
- expert_weight: float32 [512, 2], P('ep'), may hold values from 0.2 to 1
- expert_gate: bfloat16 [2048, 57344], P(None, ('ep', 'tp')), may hold values from -0.125 to 0.125
- expert_up: bfloat16 [2048, 57344], P(None, ('ep', 'tp')), may hold values from -0.125 to 0.125
- expert_down: bfloat16 [57344, 2048], P(('ep', 'tp')), may hold values from -0.0625 to 0.0625
- dense_gate: bfloat16 [2048, 5632], P('tp', 'ep'), may hold values from -0.125 to 0.125
- dense_up: bfloat16 [2048, 5632], P('tp', 'ep'), may hold values from -0.125 to 0.125
- dense_down: bfloat16 [5632, 2048], P('ep', 'tp'), may hold values from -0.078125 to 0.078125
- dense_mix: float32 [2048], P('tp'), may hold values from -2 to 2
Outputs:
- stream_out: bfloat16 [512, 2048], P('ep', 'tp')
- state_out: float32 [512, 16, 4096], P('ep', 'tp')
Inputs may be any that keep to these rules, and one draw needn't show every extreme that they name: `expert_ids`: each row names 2 different experts. In each aligned block of 32 rows no expert is named by more than 12 rows, and in some block one expert is named by exactly 12 rows.
All inputs are finite; a program needn't handle non-finite values.
Results may differ from a plain program's by a relative error of at most 0.015.
Values may be sent and summed in bfloat16 or wider, within the bound.
A program may use at most 128 MiB of HBM per device.

v0:
```python
import jax
import jax.numpy as jnp
from jax import lax
from jax.sharding import PartitionSpec as P

HEAD = 64
HEADS = 16
GROUPS = 4
NSTATE = 64
EXPERTS = 8
TOP_K = 2
CAP = 12


EPS = 1e-06


def rms_scale(values):
    return values * lax.rsqrt(jnp.mean(values * values, axis=-1, keepdims=True) + EPS)


def short_conv(past_rows, newest, tap_weights, along):
    window = jnp.concatenate([past_rows, jnp.expand_dims(newest, along)], axis=along).astype(
        jnp.float32
    )
    return jax.nn.silu(jnp.sum(window * tap_weights, axis=along))


def mix_heads(
    stream,
    mixer_gain,
    gate_proj,
    input_proj,
    state_maps,
    step_proj,
    step_bias,
    decay_rate,
    input_taps,
    map_taps,
    input_past,
    map_past,
    head_state,
    skip_gain,
    inner_gain,
):
    row_count = stream.shape[0]
    normed = (rms_scale(stream.astype(jnp.float32)) * mixer_gain).astype(jnp.bfloat16)
    gate_in = jnp.dot(normed, gate_proj, preferred_element_type=jnp.float32).astype(jnp.bfloat16)
    input_new = jnp.dot(normed, input_proj, preferred_element_type=jnp.float32).astype(jnp.bfloat16)
    map_new = jnp.stack(
        [
            jnp.dot(normed, state_maps[0], preferred_element_type=jnp.float32),
            jnp.dot(normed, state_maps[1], preferred_element_type=jnp.float32),
        ],
        axis=1,
    ).astype(jnp.bfloat16)
    step_size = jax.nn.softplus(
        jnp.dot(normed, step_proj, preferred_element_type=jnp.float32) + step_bias
    )
    conv_in = short_conv(input_past, input_new, input_taps, 1)
    conv_map = short_conv(map_past, map_new, map_taps, 2)
    head_count = step_size.shape[1]
    per_group = HEADS // GROUPS
    group_count = head_count // per_group
    write_map = jnp.repeat(
        conv_map[:, 0].reshape(row_count, group_count, NSTATE), per_group, axis=1
    )
    read_map = jnp.repeat(conv_map[:, 1].reshape(row_count, group_count, NSTATE), per_group, axis=1)
    values = conv_in.reshape(row_count, head_count, HEAD)
    decay_now = jnp.exp(-decay_rate * step_size)
    state_old = head_state.reshape(row_count, head_count, HEAD, NSTATE)
    state_new = (
        decay_now[:, :, None, None] * state_old
        + (step_size[:, :, None] * values)[:, :, :, None] * write_map[:, :, None, :]
    )
    gated = jnp.sum(state_new * read_map[:, :, None, :], axis=3) + skip_gain[:, None] * values
    gated = gated.reshape(row_count, head_count * HEAD) * jax.nn.silu(gate_in.astype(jnp.float32))
    inner_out = (
        rms_scale(gated.reshape(row_count, group_count, -1)).reshape(row_count, -1) * inner_gain
    )
    return (inner_out.astype(jnp.bfloat16), state_new.reshape(row_count, head_count, HEAD * NSTATE))


def local(
    stream,
    mixer_gain,
    gate_proj,
    input_proj,
    state_maps,
    step_proj,
    step_bias,
    decay_rate,
    input_taps,
    map_taps,
    input_past,
    map_past,
    head_state,
    skip_gain,
    inner_gain,
    mixer_out,
    channel_gain,
    expert_ids,
    expert_weight,
    expert_gate,
    expert_up,
    expert_down,
    dense_gate,
    dense_up,
    dense_down,
    dense_mix,
):
    inner_out, state_out = mix_heads(
        stream,
        mixer_gain,
        gate_proj,
        input_proj,
        state_maps,
        step_proj,
        step_bias,
        decay_rate,
        input_taps,
        map_taps,
        input_past,
        map_past,
        head_state,
        skip_gain,
        inner_gain,
    )
    partial_out = jnp.dot(inner_out, mixer_out, preferred_element_type=jnp.float32)
    mixed = lax.psum(partial_out.astype(jnp.bfloat16), "tp").astype(jnp.float32)
    hidden_mid = stream.astype(jnp.float32) + mixed
    ffn_in = (rms_scale(hidden_mid) * channel_gain).astype(jnp.bfloat16)
    row_count, feature_count = ffn_in.shape
    half_width = feature_count // lax.axis_size("tp")
    offset = lax.axis_index("tp") * half_width
    own_half = lax.dynamic_slice_in_dim(ffn_in, offset, half_width, 1)
    kept = lax.dynamic_slice_in_dim(hidden_mid, offset, half_width, 1)
    expert_span = lax.axis_size("ep") // EXPERTS
    flat_ids = expert_ids.reshape(-1)
    hit_table = (flat_ids[:, None] == jnp.arange(EXPERTS, dtype=jnp.int32)[None, :]).astype(
        jnp.int32
    )
    slot_rank = jnp.sum(jnp.cumsum(hit_table, axis=0) * hit_table, axis=1) - 1
    slot_index = flat_ids * CAP + slot_rank
    slot_table = (
        slot_index[:, None] == jnp.arange(EXPERTS * CAP, dtype=jnp.int32)[None, :]
    ).astype(jnp.float32)
    slot_table = slot_table.reshape(row_count, TOP_K, EXPERTS * CAP)
    chosen = jnp.sum(slot_table, axis=1).astype(jnp.bfloat16)
    outgoing = jnp.dot(chosen.T, ffn_in, preferred_element_type=jnp.float32).astype(jnp.bfloat16)
    outgoing = jnp.repeat(outgoing.reshape(EXPERTS, CAP, feature_count), expert_span, axis=0)
    received = lax.all_to_all(outgoing, "ep", split_axis=0, concat_axis=0, tiled=True)
    sources, item_count, width_in = received.shape
    flat_rows = received.reshape(sources * item_count, width_in)
    gate_val = jnp.dot(flat_rows, expert_gate, preferred_element_type=jnp.float32)
    up_val = jnp.dot(flat_rows, expert_up, preferred_element_type=jnp.float32)
    act = (jax.nn.silu(gate_val) * up_val).astype(jnp.bfloat16)
    share = jnp.dot(act, expert_down, preferred_element_type=jnp.float32).reshape(
        sources, item_count, width_in
    )
    halves = lax.psum_scatter(
        share.astype(jnp.bfloat16), "tp", scatter_dimension=2, tiled=True
    ).astype(jnp.float32)
    results = lax.all_to_all(
        halves.astype(jnp.bfloat16), "ep", split_axis=0, concat_axis=0, tiled=True
    ).astype(halves.dtype)
    piece = lax.all_gather(own_half, "ep", axis=0, tiled=True)
    gathered = jnp.concatenate(
        [
            jnp.dot(piece, dense_gate, preferred_element_type=jnp.float32),
            jnp.dot(piece, dense_up, preferred_element_type=jnp.float32),
        ],
        axis=1,
    )
    summed = lax.psum(gathered.astype(jnp.bfloat16), "tp").astype(jnp.float32)
    unit_count = dense_gate.shape[1]
    dense_act = (jax.nn.silu(summed[:, :unit_count]) * summed[:, unit_count:]).astype(jnp.bfloat16)
    mix_scale = jax.nn.sigmoid(dense_mix)
    per_expert = jnp.sum(results.reshape(EXPERTS, expert_span, CAP, half_width), axis=1)
    per_expert = per_expert.reshape(EXPERTS * CAP, half_width)
    combine = jnp.sum(slot_table * expert_weight[:, :, None], axis=1)
    routed = jnp.dot(combine, per_expert, precision=lax.Precision.HIGHEST)
    dense_out = lax.psum_scatter(
        jnp.dot(dense_act, dense_down, preferred_element_type=jnp.float32) * mix_scale,
        "ep",
        scatter_dimension=0,
        tiled=True,
    )
    updated = kept + routed + dense_out
    return (updated.astype(jnp.bfloat16), state_out)


def solution(mesh):
    placed = (
        P("ep", None),
        P(),
        P(None, "tp"),
        P(None, "tp"),
        P(None, None, "tp"),
        P(None, "tp"),
        P("tp"),
        P("tp"),
        P(None, "tp"),
        P(None, None, "tp"),
        P("ep", None, "tp"),
        P("ep", None, None, "tp"),
        P("ep", "tp", None),
        P("tp"),
        P("tp"),
        P("tp", None),
        P(),
        P("ep", None),
        P("ep", None),
        P(None, ("ep", "tp")),
        P(None, ("ep", "tp")),
        P(("ep", "tp"), None),
        P("tp", "ep"),
        P("tp", "ep"),
        P("ep", "tp"),
        P("tp"),
    )
    return jax.shard_map(
        local,
        mesh=mesh,
        in_specs=placed,
        out_specs=(P("ep", "tp"), P("ep", "tp", None)),
        check_vma=False,
    )
```

profile of v0, /device:TPU:0, one launch (start us, length us, event | category | flops | bytes accessed | tf_op | source)
XLA Modules:
  0.0 255.8 jit_solution(14987095764911211181)
XLA Ops:
  7.2 1.2 fusion.14
  8.5 1.4 fusion.5
  10.0 1.4 fusion.6
  11.4 2.2 fusion.4
  14.7 7.9 %reshape.146 = f32[32,8,64,64]{3,2,1,0:T(8,128)} reshape(f32[32,8,4096]{2,1,0:T(8,128)} %param.38) | data formatting | bytes 8388608 | tf_op jit(solution)/shard_map/reshape | solution.py:71
  22.7 8.6 %broadcast_multiply_fusion = (f32[32,8,64,64]{3,2,1,0:T(8,128)}, f32[32,8,64]{2,1,0:T(8,128)S(1)}) fusion(f32[32,8,64]{2,1,0:T(8,128)S(1)} %bitcast.40, f32[32,8,64]{2,1,0:T(8,128)S(1)} %multiply_multiply_fusion, f32[32,8,64]{2,1,0:T(8,128)S(1)} %bitcast.41, f32[32,8,64,64]{3,2,1,0:T(8,128)} %reshape.146, f32[32,8]{1,0:T(8,128)S(1)} %copy.64), kind=kLoop, calls=%fused_computation.2 | loop fusion | flops 5226496 | bytes 8651776 | tf_op jit(solution)/shard_map/mul | solution.py:74
  31.6 2.1 fusion.27
  34.1 1.1 convolution_convert_fusion.2
  36.1 19.9 %all-reduce.3.cloned.1.call-done = bf16[32,2048]{1,0:T(8,128)(2,1)} async-done(((bf16[32,2048]{1,0:T(8,128)(2,1)}), bf16[32,2048]{1,0:T(8,128)(2,1)}) %all-reduce.3.cloned.1.call-update) | async-done | bytes 131088 | tf_op jit(solution)/shard_map/psum | solution.py:130
  56.0 1.1 convert_add_fusion
  57.1 1.0 multiply_convert_fusion
  58.1 0.3 convolution_convert_fusion.1
  58.5 1.1 broadcast_in_dim.11
  59.6 6.8 %all-to-all-start = ((bf16[16,12,2048]{2,1,0:T(8,128)(2,1)}), bf16[16,12,2048]{2,1,0:T(8,128)(2,1)S(1)}, u32[]{:S(2)}, u32[]{:S(2)}) async-start(bf16[16,12,2048]{2,1,0:T(8,128)(2,1)} %bitcast.7), calls=%async_computation | async-start | bytes 2097152 | tf_op jit(solution)/shard_map/all_to_all | solution.py:152
  66.5 0.6 constant_dynamic-slice_fusion
  67.2 24.9 %all-to-all-done = bf16[16,12,2048]{2,1,0:T(8,128)(2,1)S(1)} async-done(((bf16[16,12,2048]{2,1,0:T(8,128)(2,1)}), bf16[16,12,2048]{2,1,0:T(8,128)(2,1)S(1)}, u32[]{:S(2)}, u32[]{:S(2)}) %all-to-all-start) | async-done | bytes 786464 | tf_op jit(solution)/shard_map/all_to_all | solution.py:152
  92.3 5.8 %fusion.28 = f32[192,1792]{1,0:T(8,128)} fusion(bf16[192,2048]{1,0:T(8,128)(2,1)S(1)} %reshape.149, bf16[2048,1792]{1,0:T(8,128)(2,1)} %param.45), kind=kOutput, calls=%fused_computation.69 | convolution fusion | flops 1409286144 | bytes 9502720 | tf_op jit(solution)/shard_map/dot_general | solution.py:155
  98.0 30.7 %all-gather.2.cloned.1.call-done = bf16[512,1024]{1,0:T(8,128)(2,1)} async-done(((bf16[32,1024]{1,0:T(8,128)(2,1)}), bf16[512,1024]{1,0:T(8,128)(2,1)}) %all-gather.2.cloned.1.call-update) | async-done | bytes 1048592 | tf_op jit(solution)/shard_map/all_gather | solution.py:167
  128.7 2.1 convolution_convert_fusion.3
  130.9 0.6 convolution_convert_fusion.4
  131.4 0.9 pad_maximum_fusion
  132.4 9.4 %convolution_convert_fusion = bf16[192,2048]{1,0:T(8,128)(2,1)S(1)} fusion(bf16[1792,2048]{1,0:T(8,128)(2,1)} %param.47, bf16[192,2048]{1,0:T(8,128)(2,1)S(1)} %reshape.149, bf16[2048,1792]{1,0:T(8,128)(2,1)} %param.46, f32[192,1792]{1,0:T(8,128)} %fusion.28), kind=kOutput, calls=%fused_computation.5 | convolution fusion | flops 2821029888 | bytes 17629184 | tf_op jit(solution)/shard_map/dot_general | solution.py:158
  141.8 1.2 convert_element_type.94
  143.2 7.0 %all-reduce.5.cloned.1.call-done = bf16[512,704]{0,1:T(8,128)(2,1)} async-done(((bf16[512,704]{0,1:T(8,128)(2,1)}), bf16[512,704]{0,1:T(8,128)(2,1)}) %all-reduce.5.cloned.1.call-update) | async-done | bytes 720912 | tf_op jit(solution)/shard_map/psum | solution.py:175
  150.3 1.3 convert_element_type.95
  151.6 3.3 %convolution_multiply_fusion.1 = f32[512,1024]{1,0:T(8,128)} fusion(bf16[352,1024]{1,0:T(8,128)(2,1)} %param.50, f32[1024]{0:T(1024)S(1)} %add_divide_fusion, f32[512,704]{0,1:T(8,128)S(1)} %convert_element_type.95), kind=kOutput, calls=%fused_computation.8 | convolution fusion | flops 370704384 | bytes 4263936 | tf_op jit(solution)/shard_map/dot_general | solution.py:184
  154.9 7.9 %mul.279 = f32[32,8,4096]{2,1,0:T(8,128)} reshape(f32[32,8,64,64]{3,2,1,0:T(8,128)} %get-tuple-element.6) | data formatting | bytes 8388608 | tf_op jit(solution)/shard_map/mul | solution.py:74
  162.8 6.8 %all-to-all-start.1 = ((bf16[16,12,1024]{2,1,0:T(8,128)(2,1)}), bf16[16,12,1024]{2,1,0:T(8,128)(2,1)S(1)}, u32[]{:S(2)}, u32[]{:S(2)}) async-start(bf16[16,12,1024]{2,1,0:T(8,128)(2,1)} %reduce-scatter.3.cloned.1.call-done), calls=%async_computation.2 | async-start | bytes 1048576 | tf_op jit(solution)/shard_map/all_to_all | solution.py:164
  169.6 6.8 %multiply_add_fusion = f32[32,8,4096]{2,1,0:T(8,128)} fusion(f32[32,8,4096]{2,1,0:T(8,128)} %mul.279, f32[32,8,4096]{2,1,0:T(8,128)} %param.38, f32[32,8]{1,0:T(8,128)S(1)} %copy.64), kind=kLoop, calls=%fused_computation.1 | loop fusion | flops 2097152 | bytes 12583936 | tf_op jit(solution)/shard_map/add | solution.py:73
  176.4 12.7 %all-to-all-done.1 = bf16[16,12,1024]{2,1,0:T(8,128)(2,1)S(1)} async-done(((bf16[16,12,1024]{2,1,0:T(8,128)(2,1)}), bf16[16,12,1024]{2,1,0:T(8,128)(2,1)S(1)}, u32[]{:S(2)}, u32[]{:S(2)}) %all-to-all-start.1) | async-done | bytes 393248 | tf_op jit(solution)/shard_map/all_to_all | solution.py:164
  189.3 58.1 %reduce-scatter.5.cloned.1.call-done = f32[32,1024]{1,0:T(8,128)} async-done(((f32[512,1024]{1,0:T(8,128)}), f32[32,1024]{1,0:T(8,128)}) %reduce-scatter.5.cloned.1.call-update) | async-done | bytes 131088 | tf_op jit(solution)/shard_map/reduce_scatter | solution.py:183
  247.4 1.9 fusion.2
  (91 shorter events, 3.5 us)
Async XLA Ops:
  7.2 26.9 %copy-start = (bf16[512,2048]{1,0:T(8,128)(2,1)S(1)}, bf16[512,2048]{1,0:T(8,128)(2,1)}, u32[]{:S(2)}) copy-start(bf16[512,2048]{1,0:T(8,128)(2,1)} %param.41) | copy-start | bytes 6291460
  7.2 6.4 %copy-start.6 = (f32[4,512]{1,0:T(4,128)S(1)}, f32[4,512]{1,0:T(4,128)}, u32[]{:S(2)}) copy-start(f32[4,512]{1,0:T(4,128)} %param.34) | copy-start | bytes 24580
  7.2 6.4 %copy-start.3 = (bf16[32,3,512]{2,0,1:T(8,128)(2,1)S(1)}, bf16[32,3,512]{2,0,1:T(8,128)(2,1)}, u32[]{:S(2)}) copy-start(bf16[32,3,512]{2,0,1:T(8,128)(2,1)} %param.36) | copy-start | bytes 294916
  7.2 48.8 %all-reduce.3.cloned.1.call-start = ((), (), s32[]{:S(2)}) async-start(), calls=%async_computation.4 | async-start | bytes 262144 | tf_op jit(solution)/shard_map/psum | solution.py:130
  8.4 5.3 %copy-start.17 = (f32[8]{0:T(128)S(1)}, f32[8]{0:T(128)}, u32[]{:S(2)}) copy-start(f32[8]{0:T(128)} %param.33) | copy-start | bytes 100
  8.4 5.3 %copy-start.2 = (bf16[32,2048]{1,0:T(8,128)(2,1)S(1)}, bf16[32,2048]{1,0:T(8,128)(2,1)}, u32[]{:S(2)}) copy-start(bf16[32,2048]{1,0:T(8,128)(2,1)} %param.26) | copy-start | bytes 393220
  8.5 5.3 %copy-start.5 = (f32[2048]{0:T(1024)S(1)}, f32[2048]{0:T(1024)}, u32[]{:S(2)}) copy-start(f32[2048]{0:T(1024)} %param.27) | copy-start | bytes 24580
  8.5 5.3 %copy-start.16 = (bf16[2048,8]{0,1:T(8,128)(2,1)S(1)}, bf16[2048,8]{0,1:T(8,128)(2,1)}, u32[]{:S(2)}) copy-start(bf16[2048,8]{0,1:T(8,128)(2,1)} %param.31) | copy-start | bytes 98308
  8.5 5.3 %copy-start.18 = (f32[8]{0:T(128)S(1)}, f32[8]{0:T(128)}, u32[]{:S(2)}) copy-start(f32[8]{0:T(128)} %param.32) | copy-start | bytes 100
  10.0 4.2 %copy-start.9 = (f32[2,4,128]{2,1,0:T(4,128)S(1)}, f32[2,4,128]{2,1,0:T(4,128)}, u32[]{:S(2)}) copy-start(f32[2,4,128]{2,1,0:T(4,128)} %param.35) | copy-start | bytes 12292
  10.0 4.2 %copy-start.4 = (bf16[32,2,3,128]{3,1,2,0:T(2,128)(2,1)S(1)}, bf16[32,2,3,128]{3,1,2,0:T(2,128)(2,1)}, u32[]{:S(2)}) copy-start(bf16[32,2,3,128]{3,1,2,0:T(2,128)(2,1)} %param.37) | copy-start | bytes 147460
  22.7 8.7 %copy-start.13 = (f32[8]{0:T(128)S(1)}, f32[8]{0:T(128)}, u32[]{:S(2)}) copy-start(f32[8]{0:T(128)} %param.39) | copy-start | bytes 100
  31.3 2.7 %copy-start.11 = (f32[512]{0:T(512)S(1)}, f32[512]{0:T(512)}, u32[]{:S(2)}) copy-start(f32[512]{0:T(512)} %param.40) | copy-start | bytes 6148
  33.7 1.5 copy-start.8
  33.7 2.3 copy-start.12
  33.8 23.3 %copy-start.7 = (f32[2048]{0:T(1024)S(1)}, f32[2048]{0:T(1024)}, u32[]{:S(2)}) copy-start(f32[2048]{0:T(1024)} %param.42) | copy-start | bytes 24580
  59.6 32.5 %all-to-all-start = ((bf16[16,12,2048]{2,1,0:T(8,128)(2,1)}), bf16[16,12,2048]{2,1,0:T(8,128)(2,1)S(1)}, u32[]{:S(2)}, u32[]{:S(2)}) async-start(bf16[16,12,2048]{2,1,0:T(8,128)(2,1)} %bitcast.7), calls=%async_computation | async-start | bytes 2097152 | tf_op jit(solution)/shard_map/all_to_all | solution.py:152
  66.4 62.3 %all-gather.2.cloned.1.call-start = ((), (), s32[]{:S(2)}) async-start(), calls=%async_computation.6 | async-start | bytes 1114112 | tf_op jit(solution)/shard_map/all_gather | solution.py:167
  67.2 83.1 %all-reduce.5.cloned.1.call-start = ((), (), s32[]{:S(2)}) async-start(), calls=%async_computation.7 | async-start | bytes 1441792 | tf_op jit(solution)/shard_map/psum | solution.py:175
  128.7 2.1 copy-start.14
  128.7 2.1 copy-start.15
  132.4 30.4 %reduce-scatter.3.cloned.1.call-start = ((), (), s32[]{:S(2)}) async-start(), calls=%async_computation.5 | async-start | bytes 1572864 | tf_op jit(solution)/shard_map/reduce_scatter | solution.py:161
  141.8 1.4 copy-start.10
  143.0 104.4 %reduce-scatter.5.cloned.1.call-start = ((), (), s32[]{:S(2)}) async-start(), calls=%async_computation.8 | async-start | bytes 2228224 | tf_op jit(solution)/shard_map/reduce_scatter | solution.py:183
  162.8 26.4 %all-to-all-start.1 = ((bf16[16,12,1024]{2,1,0:T(8,128)(2,1)}), bf16[16,12,1024]{2,1,0:T(8,128)(2,1)S(1)}, u32[]{:S(2)}, u32[]{:S(2)}) async-start(bf16[16,12,1024]{2,1,0:T(8,128)(2,1)} %reduce-scatter.3.cloned.1.call-done), calls=%async_computation.2 | async-start | bytes 1048576 | tf_op jit(solution)/shard_map/all_to_all | solution.py:164
  169.6 79.6 %copy-start.1 = (bf16[512,2048]{1,0:T(8,128)(2,1)S(1)}, bf16[512,2048]{1,0:T(8,128)(2,1)}, u32[]{:S(2)}) copy-start(bf16[512,2048]{1,0:T(8,128)(2,1)} %param.41) | copy-start | bytes 6291460
Sparse Core Ops, SparseCore 0:
  35.4 20.6 all-reduce.2
  70.6 58.0 all-gather.1
  132.5 17.6 all-reduce.4
  152.4 9.5 reduce-scatter.2
  164.1 83.2 reduce-scatter.4
where the time goes:
time: 257 us; the launch traced here: 256 us
  waiting for transfers between devices  153 us (60%)
  matrix products  31.8 us (12%)
  other arithmetic  21.9 us (9%)
  local copies, waits for them, and re-layouts  20.4 us (8%)
  between operations  14.3 us (6%)
  starting transfers between devices  14 us (5%)
    reduce_scatter x1, waiting for transfers between devices, local(): lax.psum_scatter(jnp.dot(dense_act, dense_down, preferred_element_type=jn...  58.1 us
    all_gather x1, waiting for transfers between devices, local(): piece = lax.all_gather(own_half, 'ep', axis=0, tiled=True)  30.7 us
    all_to_all x1, waiting for transfers between devices, local(): lax.all_to_all(outgoing, 'ep', split_axis=0, concat_axis=0, tiled=True)  24.9 us
    psum x1, waiting for transfers between devices, local(): mixed = lax.psum(partial_out.astype(jnp.bfloat16), 'tp').astype(jnp.float32)  19.9 us
    all_to_all x1, waiting for transfers between devices, local(): lax.all_to_all(halves.astype(jnp.bfloat16), 'ep', split_axis=0, concat_ax...  12.7 us
    dot_general x1, matrix products, local(): jnp.dot(act, expert_down, preferred_element_type=jnp.float32)  9.35 us
    mul x1, other arithmetic, mix_heads(): (step_size[:, :, None] * values)[:, :, :, None] * write_map[:, :, None, :]  8.62 us
    mul x1, local copies, waits for them, and re-layouts, mix_heads(): (step_size[:, :, None] * values)[:, :, :, None] * write_map[:, :, None, :]  7.9 us
  transfers between devices with their start and end apart: 7, of which 6 were waited for; matrix products, arithmetic and copies ran while one was open for 15% of the time, Pallas kernels for 0%

commit v1 on v0

v1 whole, which is shorter than its diff:
```python
import functools

import jax
import jax.numpy as jnp
from jax import lax
from jax.experimental import pallas as pl
from jax.experimental.pallas import tpu as pltpu
from jax.sharding import PartitionSpec as P

HEAD = 64
HEADS = 16
GROUPS = 4
NSTATE = 64
EXPERTS = 8
TOP_K = 2
CAP = 12


EPS = 1e-06


def rms_scale(values):
    return values * lax.rsqrt(jnp.mean(values * values, axis=-1, keepdims=True) + EPS)


def short_conv(past_rows, newest, tap_weights, along):
    window = jnp.concatenate([past_rows, jnp.expand_dims(newest, along)], axis=along).astype(
        jnp.float32
    )
    return jax.nn.silu(jnp.sum(window * tap_weights, axis=along))


def mix_heads(
    stream,
    mixer_gain,
    gate_proj,
    input_proj,
    state_maps,
    step_proj,
    step_bias,
    decay_rate,
    input_taps,
    map_taps,
    input_past,
    map_past,
    head_state,
    skip_gain,
    inner_gain,
):
    row_count = stream.shape[0]
    normed = (rms_scale(stream.astype(jnp.float32)) * mixer_gain).astype(jnp.bfloat16)
    gate_in = jnp.dot(normed, gate_proj, preferred_element_type=jnp.float32).astype(jnp.bfloat16)
    input_new = jnp.dot(normed, input_proj, preferred_element_type=jnp.float32).astype(jnp.bfloat16)
    map_new = jnp.stack(
        [
            jnp.dot(normed, state_maps[0], preferred_element_type=jnp.float32),
            jnp.dot(normed, state_maps[1], preferred_element_type=jnp.float32),
        ],
        axis=1,
    ).astype(jnp.bfloat16)
    step_size = jax.nn.softplus(
        jnp.dot(normed, step_proj, preferred_element_type=jnp.float32) + step_bias
    )
    conv_in = short_conv(input_past, input_new, input_taps, 1)
    conv_map = short_conv(map_past, map_new, map_taps, 2)
    head_count = step_size.shape[1]
    per_group = HEADS // GROUPS
    group_count = head_count // per_group
    write_map = jnp.repeat(
        conv_map[:, 0].reshape(row_count, group_count, NSTATE), per_group, axis=1
    )
    read_map = jnp.repeat(conv_map[:, 1].reshape(row_count, group_count, NSTATE), per_group, axis=1)
    values = conv_in.reshape(row_count, head_count, HEAD)
    decay_now = jnp.exp(-decay_rate * step_size)
    state_old = head_state.reshape(row_count, head_count, HEAD, NSTATE)
    state_new = (
        decay_now[:, :, None, None] * state_old
        + (step_size[:, :, None] * values)[:, :, :, None] * write_map[:, :, None, :]
    )
    gated = jnp.sum(state_new * read_map[:, :, None, :], axis=3) + skip_gain[:, None] * values
    gated = gated.reshape(row_count, head_count * HEAD) * jax.nn.silu(gate_in.astype(jnp.float32))
    inner_out = (
        rms_scale(gated.reshape(row_count, group_count, -1)).reshape(row_count, -1) * inner_gain
    )
    return (inner_out.astype(jnp.bfloat16), state_new.reshape(row_count, head_count, HEAD * NSTATE))


MESH = pl.DeviceIdType.MESH


def grid_of(ep_count):
    side = 4 if ep_count % 64 == 0 else (2 if ep_count % 4 == 0 else 1)
    return side, ep_count // (side * side)


class Place:
    def __init__(self, ep_count):
        self.side, self.line = grid_of(ep_count)
        self.ep = lax.axis_index("ep")
        self.core = lax.axis_index("tp")
        col = self.ep % self.side
        row = (self.ep // self.side) % self.side
        self.z = self.ep // (self.side * self.side)
        self.a = row * (1 - self.core) + col * self.core
        self.b = col * (1 - self.core) + row * self.core
        self.row, self.col = row, col

    def at(self, db, da, dz, core=None):
        core = self.core if core is None else core
        a = self.row * (1 - core) + self.col * core
        b = self.col * (1 - core) + self.row * core
        a = (a + da) % self.side
        b = (b + db) % self.side
        z = (self.z + dz) % self.line
        row = a * (1 - core) + b * core
        col = b * (1 - core) + a * core
        return (z * self.side + row) * self.side + col

    def near(self, db, da, dz):
        return {"ep": self.at(db, da, dz), "tp": self.core}

    def sibling(self):
        return {"ep": self.ep, "tp": 1 - self.core}

    def z_order(self):
        line = self.line
        return sorted(range(1, line), key=lambda d: (min(d, line - d), d))

    def partners(self):
        side = range(1, self.side)
        return (
            [self.near(d, 0, 0) for d in side]
            + [self.near(0, d, 0) for d in side]
            + [self.near(0, 0, d) for d in self.z_order()]
        )


def greet(targets):
    barrier = pltpu.get_barrier_semaphore()
    for target in targets:
        pl.semaphore_signal(barrier, inc=1, device_id=target, device_id_type=MESH)
    pl.semaphore_wait(barrier, len(targets))


def spread_kernel(ep_count, partial, stream, gain, meta, every, notes, kept, other, *sems):
    part_send, part_recv, note_send, note_recv, link_send, link_recv, core_send, core_recv = sems
    place = Place(ep_count)
    side, line = place.side, place.line
    half = every.shape[3]
    me = place.ep
    everyone = [{"ep": (me + d) % ep_count, "tp": place.core} for d in range(1, ep_count)]
    greet([place.sibling()] + everyone)
    sends = []

    def send(src, dst, send_sem, recv_sem, target):
        copy = pltpu.make_async_remote_copy(
            src_ref=src, dst_ref=dst, send_sem=send_sem, recv_sem=recv_sem,
            device_id=target, device_id_type=MESH,
        )
        copy.start()
        sends.append(copy)
        return copy

    swap = send(partial, other, part_send, part_recv, place.sibling())
    for d in range(1, ep_count):
        send(meta, notes.at[me], note_send.at[d - 1], note_recv.at[d - 1], everyone[d - 1])
    notes[me] = meta[...]
    swap.wait_recv()
    hidden = stream[...].astype(jnp.float32) + (
        partial[...].astype(jnp.float32) + other[...].astype(jnp.float32)
    )
    ffn_in = (rms_scale(hidden) * gain[...]).astype(jnp.bfloat16)
    first = place.core == 0
    kept[...] = jnp.where(first, hidden[:, :half], hidden[:, half:])
    every[0, me] = jnp.where(first, ffn_in[:, :half], ffn_in[:, half:])
    every[1, me] = jnp.where(first, ffn_in[:, half:], ffn_in[:, :half])

    def slot(db, da, dz):
        return ((db % side) * side + da % side) * line + dz % line

    used = [0]

    def pass_on(off, step):
        block = every.at[0, place.at(*off)]
        there = slot(*(o - s for o, s in zip(off, step)))
        send(block, block, link_send.at[used[0]], link_recv.at[there], place.near(*step))
        used[0] += 1

    def arrived(off):
        block = every.at[0, place.at(*off)]
        at = slot(*off)
        pltpu.make_async_copy(block, block, link_recv.at[at]).wait()
        send(block, every.at[1, place.at(*off)], core_send.at[at], core_recv.at[at], place.sibling())

    for dz in place.z_order():
        pass_on((0, 0, 0), (0, 0, dz))
    zs = [0] + place.z_order()
    for dz in zs:
        if dz:
            arrived((0, 0, dz))
        for d in range(1, side):
            pass_on((0, 0, dz), (0, d, 0))
        for d in range(1, side):
            pass_on((0, 0, dz), (d, 0, 0))
    for dz in zs:
        for da in range(1, side):
            arrived((0, da, dz))
            for d in range(1, side):
                pass_on((0, da, dz), (d, 0, 0))
    for dz in zs:
        for da in range(side):
            for db in range(1, side):
                arrived((db, da, dz))
    for d in range(1, ep_count):
        source = (me + ep_count - d) % ep_count
        pltpu.make_async_copy(notes.at[source], notes.at[source], note_recv.at[d - 1]).wait()
    for at in range(1, ep_count):
        dz, rest = at % line, at // line
        source = place.at(rest // side, rest % side, dz, 1 - place.core)
        block = every.at[1, source]
        pltpu.make_async_copy(block, block, core_recv.at[at]).wait()
    for copy in sends:
        copy.wait_send()


def spread(partial, stream, gain, meta):
    ep_count = lax.axis_size("ep")
    rows, width = stream.shape
    half = width // 2
    vmem = pl.BlockSpec(memory_space=pltpu.VMEM)
    dma = pltpu.SemaphoreType.DMA
    return pl.pallas_call(
        functools.partial(spread_kernel, ep_count),
        out_shape=(
            jax.ShapeDtypeStruct((2, ep_count, rows, half), jnp.bfloat16),
            jax.ShapeDtypeStruct((ep_count,) + meta.shape, jnp.float32),
            jax.ShapeDtypeStruct((rows, half), jnp.float32),
        ),
        in_specs=[vmem] * 4,
        out_specs=(vmem,) * 3,
        scratch_shapes=[
            pltpu.VMEM((rows, width), jnp.bfloat16),
            dma, dma,
            dma((ep_count,)), dma((ep_count,)),
            dma((ep_count,)), dma((ep_count,)),
            dma((ep_count,)), dma((ep_count,)),
        ],
        compiler_params=pltpu.CompilerParams(
            collective_id=1, has_side_effects=True, vmem_limit_bytes=VMEM_SMALL
        ),
        name="spread",
    )(partial, stream, gain, meta)


def collect_kernel(ep_count, own, theirs, kept, out, held, total, from_b, from_a, from_z, *sems):
    core_send, core_recv, link_send, recv_b, recv_a, recv_z = sems
    place = Place(ep_count)
    side, line = place.side, place.line
    greet([place.sibling()] + place.partners())
    zs = place.z_order() + [0]
    spots = [(db, da, dz) for dz in zs for da in range(side) for db in range(1, side)]
    spots += [(0, da, dz) for dz in zs for da in range(1, side)]
    spots += [(0, 0, dz) for dz in zs]
    sends = []

    def send(src, dst, send_sem, recv_sem, target):
        copy = pltpu.make_async_remote_copy(
            src_ref=src, dst_ref=dst, send_sem=send_sem, recv_sem=recv_sem,
            device_id=target, device_id_type=MESH,
        )
        copy.start()
        sends.append(copy)

    for at, off in enumerate(spots):
        send(
            theirs.at[place.at(*off, 1 - place.core)], held.at[at],
            core_send.at[at], core_recv.at[at], place.sibling(),
        )

    def take(ref, sem):
        pltpu.make_async_copy(ref, ref, sem).wait()
        return ref[...].astype(jnp.float32)

    for at, (db, da, dz) in enumerate(spots):
        value = own[place.at(db, da, dz)].astype(jnp.float32)
        value = value + take(held.at[at], core_recv.at[at])
        if db:
            total[at] = value.astype(jnp.bfloat16)
            send(
                total.at[at], from_b.at[db - 1, da, dz],
                link_send.at[at], recv_b.at[db - 1, da, dz], place.near(db, 0, 0),
            )
            continue
        for d in range(1, side):
            value = value + take(from_b.at[d - 1, da, dz], recv_b.at[d - 1, da, dz])
        if da:
            total[at] = value.astype(jnp.bfloat16)
            send(
                total.at[at], from_a.at[da - 1, dz],
                link_send.at[at], recv_a.at[da - 1, dz], place.near(0, da, 0),
            )
            continue
        for d in range(1, side):
            value = value + take(from_a.at[d - 1, dz], recv_a.at[d - 1, dz])
        if dz:
            total[at] = value.astype(jnp.bfloat16)
            send(
                total.at[at], from_z.at[dz - 1],
                link_send.at[at], recv_z.at[dz - 1], place.near(0, 0, dz),
            )
            continue
        for d in range(1, line):
            value = value + take(from_z.at[d - 1], recv_z.at[d - 1])
        out[...] = (kept[...] + value).astype(out.dtype)
    for copy in sends:
        copy.wait_send()


def collect(own, theirs, kept):
    ep_count = lax.axis_size("ep")
    side, line = grid_of(ep_count)
    rows, half = kept.shape
    vmem = pl.BlockSpec(memory_space=pltpu.VMEM)
    dma = pltpu.SemaphoreType.DMA
    more = max(side - 1, 1)
    block = (rows, half)
    return pl.pallas_call(
        functools.partial(collect_kernel, ep_count),
        out_shape=jax.ShapeDtypeStruct((rows, half), jnp.bfloat16),
        in_specs=[vmem] * 3,
        out_specs=vmem,
        scratch_shapes=[
            pltpu.VMEM((ep_count,) + block, jnp.bfloat16),
            pltpu.VMEM((ep_count,) + block, jnp.bfloat16),
            pltpu.VMEM((more, side, line) + block, jnp.bfloat16),
            pltpu.VMEM((more, line) + block, jnp.bfloat16),
            pltpu.VMEM((max(line - 1, 1),) + block, jnp.bfloat16),
            dma((ep_count,)), dma((ep_count,)), dma((ep_count,)),
            dma((more, side, line)), dma((more, line)), dma((max(line - 1, 1),)),
        ],
        compiler_params=pltpu.CompilerParams(
            collective_id=2, has_side_effects=True, vmem_limit_bytes=VMEM_SMALL
        ),
        name="collect",
    )(own.reshape((ep_count,) + block), theirs.reshape((ep_count,) + block), kept)


VMEM_SMALL = 40 * 1024 * 1024


def local(
    stream,
    mixer_gain,
    gate_proj,
    input_proj,
    state_maps,
    step_proj,
    step_bias,
    decay_rate,
    input_taps,
    map_taps,
    input_past,
    map_past,
    head_state,
    skip_gain,
    inner_gain,
    mixer_out,
    channel_gain,
    expert_ids,
    expert_weight,
    expert_gate,
    expert_up,
    expert_down,
    dense_gate,
    dense_up,
    dense_down,
    dense_mix,
):
    core = lax.axis_index("tp")
    first = core == 0
    swap = [(0, 1), (1, 0)]
    units = dense_gate.shape[1] // 2

    def mine(left, right):
        return jnp.where(first, left, right)

    low = jnp.concatenate([dense_gate[:, :units], dense_up[:, :units]], axis=1)
    high = jnp.concatenate([dense_gate[:, units:], dense_up[:, units:]], axis=1)
    wide_own = mine(low, high)
    wide_other = lax.ppermute(mine(high, low), "tp", swap)
    down_own = mine(dense_down[:units], dense_down[units:])
    down_other = lax.ppermute(mine(dense_down[units:], dense_down[:units]), "tp", swap)
    mix_other = lax.ppermute(dense_mix, "tp", swap)

    inner_out, state_out = mix_heads(
        stream, mixer_gain, gate_proj, input_proj, state_maps, step_proj, step_bias, decay_rate,
        input_taps, map_taps, input_past, map_past, head_state, skip_gain, inner_gain,
    )
    partial_out = jnp.dot(inner_out, mixer_out, preferred_element_type=jnp.float32)

    row_count, width = stream.shape
    half = width // 2
    named = expert_ids[:, :, None] == jnp.arange(EXPERTS, dtype=jnp.int32)
    weight = jnp.sum(jnp.where(named, expert_weight[:, :, None], 0.0), axis=1)
    hits = jnp.any(named, axis=1)
    earlier = jnp.tril(jnp.ones((row_count, row_count), jnp.bfloat16), -1)
    rank = jnp.dot(earlier, hits.astype(jnp.bfloat16), preferred_element_type=jnp.float32)
    rank = jnp.where(hits, rank, -1.0)
    lanes = -(-2 * row_count // 128) * 128
    meta = jnp.concatenate([rank.T, weight.T], axis=1)
    meta = jnp.pad(meta, ((0, 0), (0, lanes - 2 * row_count)))

    every, notes, kept = spread(
        partial_out.astype(jnp.bfloat16), stream, channel_gain[None, :], meta
    )

    ep_count = lax.axis_size("ep")
    total_rows = ep_count * row_count
    slots = ep_count * CAP
    expert = lax.axis_index("ep") // (ep_count // EXPERTS)
    notes = lax.dynamic_index_in_dim(notes, expert, 1, keepdims=False)
    rank_all = notes[:, :row_count].reshape(1, total_rows)
    weight_all = notes[:, row_count : 2 * row_count].reshape(1, total_rows)
    slot_ids = jnp.arange(slots, dtype=jnp.int32)[:, None]
    row_ids = jnp.arange(total_rows, dtype=jnp.int32)[None, :]
    match = (slot_ids // CAP == row_ids // row_count) & (
        (slot_ids % CAP).astype(jnp.float32) == rank_all
    )
    slot_weight = jnp.sum(jnp.where(match, weight_all, 0.0), axis=1, keepdims=True)
    pick = match.astype(jnp.bfloat16)
    all_own = every[0].reshape(total_rows, half)
    all_other = every[1].reshape(total_rows, half)

    def f32_dot(left, right):
        return jnp.dot(left, right, preferred_element_type=jnp.float32)

    rows_own = f32_dot(pick, all_own).astype(jnp.bfloat16)
    rows_other = f32_dot(pick, all_other).astype(jnp.bfloat16)
    rows = jnp.concatenate([mine(rows_own, rows_other), mine(rows_other, rows_own)], axis=1)
    act = (jax.nn.silu(f32_dot(rows, expert_gate)) * f32_dot(rows, expert_up)).astype(jnp.bfloat16)
    share = (f32_dot(act, expert_down) * slot_weight).astype(jnp.bfloat16)
    share_own = mine(share[:, :half], share[:, half:])
    share_other = mine(share[:, half:], share[:, :half])

    wide = f32_dot(all_own, wide_own) + f32_dot(all_other, wide_other)
    dense_act = (jax.nn.silu(wide[:, :units]) * wide[:, units:]).astype(jnp.bfloat16)

    def result(share_half, down_half, mix_half):
        spread_back = lax.dot_general(
            pick, share_half, (((0,), (0,)), ((), ())), preferred_element_type=jnp.float32
        )
        dense = f32_dot(dense_act, down_half) * jax.nn.sigmoid(mix_half)
        return (spread_back + dense).astype(jnp.bfloat16)

    updated = collect(
        result(share_own, down_own, dense_mix),
        result(share_other, down_other, mix_other),
        kept,
    )
    return (updated, state_out)


def solution(mesh):
    placed = (
        P("ep", None),
        P(),
        P(None, "tp"),
        P(None, "tp"),
        P(None, None, "tp"),
        P(None, "tp"),
        P("tp"),
        P("tp"),
        P(None, "tp"),
        P(None, None, "tp"),
        P("ep", None, "tp"),
        P("ep", None, None, "tp"),
        P("ep", "tp", None),
        P("tp"),
        P("tp"),
        P("tp", None),
        P(),
        P("ep", None),
        P("ep", None),
        P(None, ("ep", "tp")),
        P(None, ("ep", "tp")),
        P(("ep", "tp"), None),
        P("tp", "ep"),
        P("tp", "ep"),
        P("ep", "tp"),
        P("tp"),
    )
    return jax.shard_map(
        local,
        mesh=mesh,
        in_specs=placed,
        out_specs=(P("ep", "tp"), P("ep", "tp", None)),
        check_vma=False,
    )
```

time: 257 us -> 120 us (0.47)
  waiting for transfers between devices: 153 us -> 0.01 us
  Pallas kernels: 0 us -> 44.7 us
  between operations: 14.3 us -> 1.24 us
  starting transfers between devices: 14 us -> 1.13 us
  other arithmetic: 21.9 us -> 19.3 us
    reduce_scatter x2 -> x0, waiting for transfers between devices: 58.1 us -> none  [the longest x1 58.1 us: local(): lax.psum_scatter(jnp.dot(dense_act, dense_down, preferred_element_type=jn...]
    pallas_call x0 -> x2, Pallas kernels: none -> 44.7 us  [the longest x1 23.2 us: spread(): pl.pallas_call(functools.partial(spread_kernel, ep_count), out_shape=(jax...]
    all_to_all x2 -> x0, waiting for transfers between devices: 37.6 us -> none  [the longest x1 24.9 us: local(): lax.all_to_all(outgoing, 'ep', split_axis=0, concat_axis=0, tiled=True)]
    all_gather x1 -> x0, waiting for transfers between devices: 30.7 us -> none  [local(): piece = lax.all_gather(own_half, 'ep', axis=0, tiled=True)]
    psum x2 -> x0, waiting for transfers between devices: 26.9 us -> none  [the longest x1 19.9 us: local(): mixed = lax.psum(partial_out.astype(jnp.bfloat16), 'tp').astype(jnp.float32)]
    all_to_all x2 -> x0, starting transfers between devices: 13.7 us -> none  [the longest x1 6.83 us: local(): lax.all_to_all(halves.astype(jnp.bfloat16), 'ep', split_axis=0, concat_ax...]
    select_n x0 -> x4, other arithmetic: none -> 3.12 us  [the longest x2 3.11 us: mine(): return jnp.where(first, left, right)]
    dot_general x7 -> x11, matrix products: 23.2 us -> 24.7 us  [the longest x8 21 us: f32_dot(): return jnp.dot(left, right, preferred_element_type=jnp.float32)]
  transfers between devices with their start and end apart: 7 -> 3, of which waited for: 6 -> 0; matrix products, arithmetic and copies ran while one was open for 15% -> 58% of each run, Pallas kernels for 0% -> 20%
where the time goes in v1:
time: 120 us; the launch traced here: 119 us
  Pallas kernels  44.7 us (37%)
  matrix products  32.3 us (27%)
  local copies, waits for them, and re-layouts  20.3 us (17%)
  other arithmetic  19.3 us (16%)
  between operations  1.24 us (1%)
    pallas_call x1, Pallas kernels, spread(): pl.pallas_call(functools.partial(spread_kernel, ep_count), out_shape=(jax...  23.2 us
    pallas_call x1, Pallas kernels, collect(): pl.pallas_call(functools.partial(collect_kernel, ep_count), out_shape=jax...  21.5 us
    dot_general x8, matrix products, f32_dot(): return jnp.dot(left, right, preferred_element_type=jnp.float32)  21 us
    mul x1, other arithmetic, mix_heads(): (step_size[:, :, None] * values)[:, :, :, None] * write_map[:, :, None, :]  8.62 us
    reshape x1, local copies, waits for them, and re-layouts, mix_heads(): state_old = head_state.reshape(row_count, head_count, HEAD, NSTATE)  7.88 us
    mul x1, local copies, waits for them, and re-layouts, mix_heads(): (step_size[:, :, None] * values)[:, :, :, None] * write_map[:, :, None, :]  7.88 us
    add x1, other arithmetic, mix_heads(): decay_now[:, :, None, None] * state_old  6.58 us
    dot_general x2, matrix products, result(): lax.dot_general(pick, share_half, (((0,), (0,)), ((), ())), preferred_ele...  3.53 us
  transfers between devices with their start and end apart: 3, of which 0 were waited for; matrix products, arithmetic and copies ran while one was open for 58% of the time, Pallas kernels for 20%

profile of v1, /device:TPU:0, one launch (start us, length us, event | category | flops | bytes accessed | tf_op | source)
XLA Modules:
  0.0 119.0 jit_solution(8480911521833608941)
XLA Ops:
  0.6 0.6 collective-permute-start.2
  1.2 1.9 %broadcast_select_fusion.3 = bf16[176,1024]{1,0:T(8,128)(2,1)} fusion(pred[]{:T(512)S(6)} %eq.56, bf16[352,1024]{1,0:T(8,128)(2,1)} %param.50), kind=kLoop, calls=%fused_computation.48 | loop fusion | flops 180224 | bytes 1081345 | tf_op jit(solution)/shard_map/jit(_where)/select_n | solution.py:385
  3.2 1.4 %fusion.58 = (bf16[1024,176]{0,1:T(8,128)(2,1)S(1)}, bf16[1024,176]{0,1:T(8,128)(2,1)S(1)}, bf16[1024,176]{0,1:T(8,128)(2,1)S(1)}, bf16[1024,176]{0,1:T(8,128)(2,1)S(1)}) fusion(bf16[1024,352]{0,1:T(8,128)(2,1)} %param.48, bf16[1024,352]{0,1:T(8,128)(2,1)} %param.49), kind=kLoop, calls=%fused_computation.111 | loop fusion | bytes 2883584 | tf_op jit(solution)/shard_map/slice | solution.py:387
  4.8 0.6 copy-done.5
  5.4 1.2 broadcast_select_fusion
  6.6 0.5 collective-permute-start
  7.2 1.3 %fusion.4 = bf16[32,1,1,128]{3,0,2,1:T(8,128)(2,1)S(1)} fusion(bf16[2,2048,128]{2,1,0:T(8,128)(2,1)} %param.30, bf16[32,2048]{1,0:T(8,128)(2,1)S(1)} %copy-done.2, f32[2048]{0:T(1024)S(1)} %copy-done.17, f32[32]{0:T(128)S(1)} %add_rsqrt_fusion.1), kind=kOutput, calls=%fused_computation.19 | convolution fusion | flops 17043456 | bytes 671872 | tf_op jit(solution)/shard_map/dot_general | solution.py:56
  8.6 1.3 %fusion.5 = bf16[32,1,1,128]{3,0,2,1:T(8,128)(2,1)S(1)} fusion(bf16[2,2048,128]{2,1,0:T(8,128)(2,1)} %param.30, bf16[32,2048]{1,0:T(8,128)(2,1)S(1)} %copy-done.2, f32[2048]{0:T(1024)S(1)} %copy-done.17, f32[32]{0:T(128)S(1)} %add_rsqrt_fusion.1), kind=kOutput, calls=%fused_computation.20 | convolution fusion | flops 17043456 | bytes 671872 | tf_op jit(solution)/shard_map/dot_general | solution.py:57
  10.2 0.2 multiply_exponential_fusion
  11.0 2.1 %fusion.3 = bf16[32,1,512]{2,0,1:T(8,128)(2,1)S(1)} fusion(bf16[2048,512]{1,0:T(8,128)(2,1)} %param.29, bf16[32,2048]{1,0:T(8,128)(2,1)S(1)} %copy-done.2, f32[2048]{0:T(1024)S(1)} %copy-done.17, f32[32]{0:T(128)S(1)} %add_rsqrt_fusion.1), kind=kOutput, calls=%fused_computation.16 | convolution fusion | flops 67387392 | bytes 2269312 | tf_op jit(solution)/shard_map/dot_general | solution.py:53
  13.3 7.9 %reshape.182 = f32[32,8,64,64]{3,2,1,0:T(8,128)} reshape(f32[32,8,4096]{2,1,0:T(8,128)} %param.38) | data formatting | bytes 8388608 | tf_op jit(solution)/shard_map/reshape | solution.py:75
  21.3 8.6 %broadcast_multiply_fusion = (f32[32,8,64,64]{3,2,1,0:T(8,128)}, f32[32,8,64]{2,1,0:T(8,128)S(1)}) fusion(f32[32,8,64]{2,1,0:T(8,128)S(1)} %bitcast.51, f32[32,8,64]{2,1,0:T(8,128)S(1)} %multiply_multiply_fusion, f32[32,8,64]{2,1,0:T(8,128)S(1)} %bitcast.50, f32[32,8,64,64]{3,2,1,0:T(8,128)} %reshape.182, f32[32,8]{1,0:T(8,128)S(1)} %copy.42), kind=kLoop, calls=%fused_computation.2 | loop fusion | flops 5226496 | bytes 8651776 | tf_op jit(solution)/shard_map/mul | solution.py:78
  29.9 7.9 %mul.245 = f32[32,8,4096]{2,1,0:T(8,128)} reshape(f32[32,8,64,64]{3,2,1,0:T(8,128)} %get-tuple-element.18) | data formatting | bytes 8388608 | tf_op jit(solution)/shard_map/mul | solution.py:78
  37.8 6.6 %multiply_add_fusion = f32[32,8,4096]{2,1,0:T(8,128)} fusion(f32[32,8,4096]{2,1,0:T(8,128)} %mul.245, f32[32,8,4096]{2,1,0:T(8,128)} %param.38, f32[32,8]{1,0:T(8,128)S(1)} %copy.42), kind=kLoop, calls=%fused_computation.1 | loop fusion | flops 2097152 | bytes 12583936 | tf_op jit(solution)/shard_map/add | solution.py:77
  44.5 2.1 %fusion.61 = (f32[32,512]{1,0:T(8,128)S(1)}, f32[32,512]{1,0:T(8,128)S(1)}) fusion(bf16[2048,512]{1,0:T(8,128)(2,1)} %param.28, bf16[32,2048]{1,0:T(8,128)(2,1)S(1)} %copy-done.2, f32[2048]{0:T(1024)S(1)} %copy-done.17, f32[32]{0:T(128)S(1)} %add_rsqrt_fusion.1, f32[32,512]{1,0:T(8,128)S(1)} %reduce_sum.72, f32[32,512]{1,0:T(8,128)S(1)} %multiply_reduce_fusion.1, ...), kind=kOutput, calls=%fused_computation.114 | convolution fusion | flops 67600384 | bytes 2500736 | tf_op jit(solution)/shard_map/dot_general | solution.py:52
  46.9 0.2 convolution_select_fusion
  47.2 0.5 convolution_convert_fusion.partial
  47.7 23.2 %spread.1 = (bf16[2,16,32,1024]{3,2,1,0:T(8,128)(2,1)S(1)}, f32[16,8,128]{2,1,0:T(8,128)S(1)}, f32[32,1024]{1,0:T(8,128)S(1)}) custom-call(bf16[32,2048]{1,0:T(8,128)(2,1)S(1)} %convolution_convert_fusion.partial, bf16[32,2048]{1,0:T(8,128)(2,1)S(1)} %copy-done.2, f32[1,2048]{1,0:T(1,128)S(1)} %bitcast.45, f32[8,128]{1,0:T(8,128)S(1)} %select_maximum_fusion.meta), custom_call_target="tpu_custom_call" | custom-call | tf_op jit(solution)/shard_map/spread/pallas_call | solution.py:232
  71.4 0.2 select_reduce_fusion
  71.6 0.4 convolution_convert_fusion.1
  72.0 0.3 copy-done.13
  72.3 0.4 broadcast_select_fusion.2
  72.8 5.8 %fusion.13 = f32[192,1792]{1,0:T(8,128)} fusion(bf16[2048,1792]{1,0:T(8,128)(2,1)} %param.45, bf16[192,1024]{1,0:T(8,128)(2,1)S(1)} %get-tuple-element.13, bf16[192,1024]{1,0:T(8,128)(2,1)S(1)} %get-tuple-element.12), kind=kOutput, calls=%fused_computation.34 | convolution fusion | flops 1410859008 | bytes 9502720 | tf_op jit(solution)/shard_map/dot_general | solution.py:435
  78.5 10.0 %fusion = bf16[192,2048]{1,0:T(8,128)(2,1)} fusion(bf16[1792,2048]{1,0:T(8,128)(2,1)} %param.47, f32[192]{0:T(256)S(1)} %select_reduce_fusion, bf16[2048,1792]{1,0:T(8,128)(2,1)} %param.46, f32[192,1792]{1,0:T(8,128)} %fusion.13, bf16[192,1024]{1,0:T(8,128)(2,1)S(1)} %get-tuple-element.13, bf16[192,1024]{1,0:T(8,128)(2,1)S(1)} %get-tuple-element.12), kind=kOutput, calls=%fused_computation.5 | convolution fusion | flops 2822995968 | bytes 17629952 | tf_op jit(solution)/shard_map/dot_general | solution.py:435
  88.6 1.8 %fusion.16 = f32[512,1024]{1,0:T(8,128)S(1)} fusion(pred[]{:T(512)S(6)} %eq.56, bf16[192,2048]{1,0:T(8,128)(2,1)} %fusion, f32[512]{0:T(512)S(1)} %eq.53, s32[512]{0:T(512)S(1)} %add_select_fusion, f32[192]{0:T(256)S(1)} %get-tuple-element.27, s32[192]{0:T(256)S(1)} %get-tuple-element.26), kind=kOutput, calls=%fused_computation.37 | convolution fusion | flops 201818112 | bytes 2889217 | tf_op jit(solution)/shard_map/dot_general | solution.py:449
  90.4 1.7 %fusion.14 = f32[512,1024]{1,0:T(8,128)S(1)} fusion(pred[]{:T(512)S(6)} %eq.56, bf16[192,2048]{1,0:T(8,128)(2,1)} %fusion, f32[512]{0:T(512)S(1)} %eq.53, s32[512]{0:T(512)S(1)} %add_select_fusion, f32[192]{0:T(256)S(1)} %get-tuple-element.27, s32[192]{0:T(256)S(1)} %get-tuple-element.26), kind=kOutput, calls=%fused_computation.35 | convolution fusion | flops 201818112 | bytes 2889217 | tf_op jit(solution)/shard_map/dot_general | solution.py:449
  92.2 0.6 fusion.6
  92.9 1.7 %convolution_add_fusion = f32[512,352]{0,1:T(8,128)S(1)} fusion(f32[512,352]{0,1:T(8,128)S(1)} %fusion.6, bf16[512,1024]{1,0:T(8,128)(2,1)S(1)} %bitcast.47, bf16[1024,352]{0,1:T(8,128)(2,1)} %collective-permute-done), kind=kOutput, calls=%fused_computation.10 | convolution fusion | flops 369278976 | bytes 3211264 | tf_op jit(solution)/shard_map/dot_general | solution.py:435
  94.8 0.5 add_convert_fusion.1
  95.3 1.6 %add_convert_fusion = bf16[512,1024]{1,0:T(8,128)(2,1)S(1)} fusion(f32[512,1024]{1,0:T(8,128)S(1)} %fusion.14, bf16[512,176]{0,1:T(8,128)(2,1)S(1)} %fusion.20, bf16[176,1024]{1,0:T(8,128)(2,1)} %collective-permute-done.1, f32[1024]{0:T(1024)S(1)} %add_divide_fusion), kind=kOutput, calls=%fused_computation.8 | convolution fusion | flops 186122240 | bytes 3690496 | tf_op jit(solution)/shard_map/dot_general | solution.py:435
  96.9 21.5 %collect.1 = bf16[32,1024]{1,0:T(8,128)(2,1)S(1)} custom-call(bf16[16,32,1024]{2,1,0:T(8,128)(2,1)S(1)} %bitcast.43, bf16[16,32,1024]{2,1,0:T(8,128)(2,1)S(1)} %bitcast.44, f32[32,1024]{1,0:T(8,128)S(1)} %get-tuple-element.7.kept), custom_call_target="tpu_custom_call" | custom-call | tf_op jit(solution)/shard_map/collect/pallas_call | solution.py:327
  118.4 0.6 copy.49
  (98 shorter events, 2.5 us)
Async XLA Ops:
  0.6 46.6 %copy-start = (bf16[512,2048]{1,0:T(8,128)(2,1)S(1)}, bf16[512,2048]{1,0:T(8,128)(2,1)}, u32[]{:S(2)}) copy-start(bf16[512,2048]{1,0:T(8,128)(2,1)} %param.41) | copy-start | bytes 6291460
  0.6 92.2 %collective-permute-start.2 = (f32[1024]{0:T(1024)}, f32[1024]{0:T(1024)S(1)}, u32[]{:S(2)}, u32[]{:S(2)}) collective-permute-start(f32[1024]{0:T(1024)} %param.51), channel_id=1, source_target_pairs={{0,1},{1,0},{2,3},{3,2},{4,5},{5,4},{6,7},{7,6},{8,9},{9,8},{10,11... | collective-permute-start | bytes 12296 | tf_op jit(solution)/shard_map/ppermute | solution.py:393
  3.1 3.9 %copy-start.2 = (bf16[32,2048]{1,0:T(8,128)(2,1)S(1)}, bf16[32,2048]{1,0:T(8,128)(2,1)}, u32[]{:S(2)}) copy-start(bf16[32,2048]{1,0:T(8,128)(2,1)} %stream.1) | copy-start | bytes 393220
  3.1 4.1 %copy-start.17 = (f32[2048]{0:T(1024)S(1)}, f32[2048]{0:T(1024)}, u32[]{:S(2)}) copy-start(f32[2048]{0:T(1024)} %param.27) | copy-start | bytes 24580
  3.1 92.1 %collective-permute-start.1 = (bf16[176,1024]{1,0:T(8,128)(2,1)}, bf16[176,1024]{1,0:T(8,128)(2,1)}, u32[]{:S(2)}, u32[]{:S(2)}) collective-permute-start(bf16[176,1024]{1,0:T(8,128)(2,1)} %broadcast_select_fusion.3), channel_id=1, source_target_pairs={{0,1},{1,0},{2,3},{3,2},{4,5},{5,4},{6,7},{7,6},{8,9},{9,8},{10,11... | collective-permute-start | bytes 1081352 | tf_op jit(solution)/shard_map/ppermute | solution.py:392
  4.6 0.7 copy-start.5
  4.7 1.9 %copy-start.7 = (bf16[1024,176]{0,1:T(8,128)(2,1)}, bf16[1024,176]{0,1:T(8,128)(2,1)S(1)}, u32[]{:S(2)}) copy-start(bf16[1024,176]{0,1:T(8,128)(2,1)S(1)} %get-tuple-element.15) | copy-start | bytes 1081348
  4.7 1.9 %copy-start.9 = (bf16[1024,176]{0,1:T(8,128)(2,1)}, bf16[1024,176]{0,1:T(8,128)(2,1)S(1)}, u32[]{:S(2)}) copy-start(bf16[1024,176]{0,1:T(8,128)(2,1)S(1)} %get-tuple-element.28) | copy-start | bytes 1081348
  4.7 1.9 %copy-start.11 = (bf16[1024,176]{0,1:T(8,128)(2,1)}, bf16[1024,176]{0,1:T(8,128)(2,1)S(1)}, u32[]{:S(2)}) copy-start(bf16[1024,176]{0,1:T(8,128)(2,1)S(1)} %get-tuple-element.29) | copy-start | bytes 1081348
  4.7 5.2 %copy-start.26 = (f32[8]{0:T(128)S(1)}, f32[8]{0:T(128)}, u32[]{:S(2)}) copy-start(f32[8]{0:T(128)} %param.33) | copy-start | bytes 100
  4.7 5.2 %copy-start.21 = (s32[32,2]{0,1:T(2,128)S(1)}, s32[32,2]{0,1:T(2,128)}, u32[]{:S(2)}) copy-start(s32[32,2]{0,1:T(2,128)} %param.43) | copy-start | bytes 772
  4.7 5.3 %copy-start.19 = (f32[2,4,128]{2,1,0:T(4,128)S(1)}, f32[2,4,128]{2,1,0:T(4,128)}, u32[]{:S(2)}) copy-start(f32[2,4,128]{2,1,0:T(4,128)} %param.35) | copy-start | bytes 12292
  4.7 5.3 %copy-start.24 = (f32[8]{0:T(128)S(1)}, f32[8]{0:T(128)}, u32[]{:S(2)}) copy-start(f32[8]{0:T(128)} %param.39) | copy-start | bytes 100
  4.7 5.4 %copy-start.23 = (f32[32,2]{0,1:T(2,128)S(1)}, f32[32,2]{0,1:T(2,128)}, u32[]{:S(2)}) copy-start(f32[32,2]{0,1:T(2,128)} %param.44) | copy-start | bytes 772
  4.7 5.4 %copy-start.25 = (bf16[2048,8]{0,1:T(8,128)(2,1)S(1)}, bf16[2048,8]{0,1:T(8,128)(2,1)}, u32[]{:S(2)}) copy-start(bf16[2048,8]{0,1:T(8,128)(2,1)} %param.31) | copy-start | bytes 98308
  4.8 5.4 %copy-start.27 = (f32[8]{0:T(128)S(1)}, f32[8]{0:T(128)}, u32[]{:S(2)}) copy-start(f32[8]{0:T(128)} %param.32) | copy-start | bytes 100
  5.4 5.1 %copy-start.16 = (bf16[32,2,3,128]{3,1,2,0:T(2,128)(2,1)S(1)}, bf16[32,2,3,128]{3,1,2,0:T(2,128)(2,1)}, u32[]{:S(2)}) copy-start(bf16[32,2,3,128]{3,1,2,0:T(2,128)(2,1)} %param.37) | copy-start | bytes 147460
  6.6 86.3 %collective-permute-start = (bf16[1024,352]{0,1:T(8,128)(2,1)}, bf16[1024,352]{0,1:T(8,128)(2,1)}, u32[]{:S(2)}, u32[]{:S(2)}) collective-permute-start(bf16[1024,352]{0,1:T(8,128)(2,1)} %broadcast_select_fusion), channel_id=1, source_target_pairs={{0,1},{1,0},{2,3},{3,2},{4,5},{5,4},{6,7},{7,6},{8,9},{9,8},{10,11... | collective-permute-start | bytes 2162696 | tf_op jit(solution)/shard_map/ppermute | solution.py:390
  8.5 4.6 %copy-start.15 = (bf16[32,3,512]{2,0,1:T(8,128)(2,1)S(1)}, bf16[32,3,512]{2,0,1:T(8,128)(2,1)}, u32[]{:S(2)}) copy-start(bf16[32,3,512]{2,0,1:T(8,128)(2,1)} %param.36) | copy-start | bytes 294916
  8.6 4.6 %copy-start.18 = (f32[4,512]{1,0:T(4,128)S(1)}, f32[4,512]{1,0:T(4,128)}, u32[]{:S(2)}) copy-start(f32[4,512]{1,0:T(4,128)} %param.34) | copy-start | bytes 24580
  44.4 2.8 %copy-start.22 = (f32[512]{0:T(512)S(1)}, f32[512]{0:T(512)}, u32[]{:S(2)}) copy-start(f32[512]{0:T(512)} %param.40) | copy-start | bytes 6148
  44.5 3.2 %copy-start.3 = (f32[2048]{0:T(1024)S(1)}, f32[2048]{0:T(1024)}, u32[]{:S(2)}) copy-start(f32[2048]{0:T(1024)} %param.42) | copy-start | bytes 24580
  71.4 1.0 copy-start.13
  88.5 3.6 %copy-start.6 = (bf16[1024,176]{0,1:T(8,128)(2,1)S(1)}, bf16[1024,176]{0,1:T(8,128)(2,1)}, u32[]{:S(2)}) copy-start(bf16[1024,176]{0,1:T(8,128)(2,1)} %copy-done.5) | copy-start | bytes 1081348
  88.5 3.6 %copy-start.8 = (bf16[1024,176]{0,1:T(8,128)(2,1)S(1)}, bf16[1024,176]{0,1:T(8,128)(2,1)}, u32[]{:S(2)}) copy-start(bf16[1024,176]{0,1:T(8,128)(2,1)} %copy-done.7) | copy-start | bytes 1081348
  88.5 3.6 %copy-start.10 = (bf16[1024,176]{0,1:T(8,128)(2,1)S(1)}, bf16[1024,176]{0,1:T(8,128)(2,1)}, u32[]{:S(2)}) copy-start(bf16[1024,176]{0,1:T(8,128)(2,1)} %copy-done.9) | copy-start | bytes 1081348
  88.5 3.6 %copy-start.12 = (bf16[1024,176]{0,1:T(8,128)(2,1)S(1)}, bf16[1024,176]{0,1:T(8,128)(2,1)}, u32[]{:S(2)}) copy-start(bf16[1024,176]{0,1:T(8,128)(2,1)} %copy-done.11) | copy-start | bytes 1081348
  88.5 3.6 %copy-start.14 = (bf16[1,16,32,1024]{3,2,1,0:T(8,128)(2,1)S(1)}, bf16[1,16,32,1024]{3,2,1,0:T(8,128)(2,1)}, u32[]{:S(2)}) copy-start(bf16[1,16,32,1024]{3,2,1,0:T(8,128)(2,1)} %copy-done.13) | copy-start | bytes 3145732
  92.2 0.7 copy-start.20
  92.8 1.9 %copy-start.4 = (bf16[352,1024]{1,0:T(8,128)(2,1)S(1)}, bf16[352,1024]{1,0:T(8,128)(2,1)}, u32[]{:S(2)}) copy-start(bf16[352,1024]{1,0:T(8,128)(2,1)} %param.50) | copy-start | bytes 2162692
  95.2 23.8 %copy-start.1 = (bf16[512,2048]{1,0:T(8,128)(2,1)S(1)}, bf16[512,2048]{1,0:T(8,128)(2,1)}, u32[]{:S(2)}) copy-start(bf16[512,2048]{1,0:T(8,128)(2,1)} %param.41) | copy-start | bytes 6291460

commit v2 on v1

--- a/solution.py
+++ b/solution.py
@@ -28,6 +28,68 @@
         jnp.float32
     )
     return jax.nn.silu(jnp.sum(window * tap_weights, axis=along))
+
+
+def three_parts(value):
+    high = value.astype(jnp.bfloat16)
+    rest = value - high.astype(jnp.float32)
+    middle = rest.astype(jnp.bfloat16)
+    return high, middle, (rest - middle.astype(jnp.float32)).astype(jnp.bfloat16)
+
+
+def state_kernel(state, fed, write, read_by, decay, state_out, read, picks):
+    lanes = state.shape[1]
+
+    @pl.when(pl.program_id(0) == 0)
+    def _():
+        rows_of = lax.broadcasted_iota(jnp.int32, picks.shape, 0)
+        owner = lax.broadcasted_iota(jnp.int32, picks.shape, 1) // NSTATE
+        picks[...] = jnp.where(rows_of == owner, 1.0, 0.0).astype(jnp.bfloat16)
+
+    width = 4 * 128
+    copies = width // NSTATE
+    fed_parts = three_parts(fed[...])
+    write_wide = jnp.concatenate([write[...]] * copies, axis=1)
+    read_wide = jnp.concatenate([read_by[...]] * copies, axis=1)
+    decay_wide = jnp.concatenate([decay[...]] * (width // 128), axis=1)
+    total = jnp.zeros(read.shape, jnp.float32)
+    for at in range(0, lanes, width):
+        cut = slice(at, at + width)
+        pick = picks[:, cut]
+        fed_wide = sum(
+            jnp.dot(part, pick, preferred_element_type=jnp.float32) for part in fed_parts[::-1]
+        )
+        value = decay_wide * state[:, cut] + fed_wide * write_wide
+        state_out[:, cut] = value
+        for part in three_parts(value * read_wide):
+            total = total + lax.dot_general(
+                part, pick, (((1,), (1,)), ((), ())), preferred_element_type=jnp.float32
+            )
+    read[...] = total
+
+
+def step_state(state, fed, write, read_by, decay):
+    flat, lanes = state.shape
+    rows = 64
+
+    def block(array):
+        return pl.BlockSpec((rows, array.shape[1]), lambda i: (i, 0))
+
+    return pl.pallas_call(
+        state_kernel,
+        grid=(flat // rows,),
+        out_shape=(
+            jax.ShapeDtypeStruct(state.shape, jnp.float32),
+            jax.ShapeDtypeStruct(fed.shape, jnp.float32),
+        ),
+        in_specs=[block(x) for x in (state, fed, write, read_by, decay)],
+        out_specs=(block(state), block(fed)),
+        scratch_shapes=[pltpu.VMEM((HEAD, lanes), jnp.bfloat16)],
+        compiler_params=pltpu.CompilerParams(
+            dimension_semantics=("arbitrary",), vmem_limit_bytes=16 * 1024 * 1024
+        ),
+        name="state",
+    )(state, fed, write, read_by, decay)
 
 
 def mix_heads(
@@ -66,23 +128,32 @@
     head_count = step_size.shape[1]
     per_group = HEADS // GROUPS
     group_count = head_count // per_group
-    write_map = jnp.repeat(
-        conv_map[:, 0].reshape(row_count, group_count, NSTATE), per_group, axis=1
-    )
-    read_map = jnp.repeat(conv_map[:, 1].reshape(row_count, group_count, NSTATE), per_group, axis=1)
     values = conv_in.reshape(row_count, head_count, HEAD)
     decay_now = jnp.exp(-decay_rate * step_size)
-    state_old = head_state.reshape(row_count, head_count, HEAD, NSTATE)
-    state_new = (
-        decay_now[:, :, None, None] * state_old
-        + (step_size[:, :, None] * values)[:, :, :, None] * write_map[:, :, None, :]
-    )
-    gated = jnp.sum(state_new * read_map[:, :, None, :], axis=3) + skip_gain[:, None] * values
+    flat = row_count * head_count
+
+    def by_head(maps):
+        maps = maps.reshape(row_count, group_count, 1, NSTATE)
+        return jnp.broadcast_to(
+            maps, (row_count, group_count, per_group, NSTATE)
+        ).reshape(flat, NSTATE)
+
+    state_new, read = step_state(
+        head_state.reshape(flat, HEAD * NSTATE),
+        (step_size[:, :, None] * values).reshape(flat, HEAD),
+        by_head(conv_map[:, 0]),
+        by_head(conv_map[:, 1]),
+        jnp.broadcast_to(decay_now[:, :, None], (row_count, head_count, 128)).reshape(flat, 128),
+    )
+    gated = read.reshape(row_count, head_count, HEAD) + skip_gain[:, None] * values
     gated = gated.reshape(row_count, head_count * HEAD) * jax.nn.silu(gate_in.astype(jnp.float32))
     inner_out = (
         rms_scale(gated.reshape(row_count, group_count, -1)).reshape(row_count, -1) * inner_gain
     )
-    return (inner_out.astype(jnp.bfloat16), state_new.reshape(row_count, head_count, HEAD * NSTATE))
+    return (
+        inner_out.astype(jnp.bfloat16),
+        state_new.reshape(row_count, head_count, HEAD * NSTATE),
+    )
 
 
 MESH = pl.DeviceIdType.MESH
@@ -246,7 +317,7 @@
             dma((ep_count,)), dma((ep_count,)),
         ],
         compiler_params=pltpu.CompilerParams(
-            collective_id=1, has_side_effects=True, vmem_limit_bytes=VMEM_SMALL
+            collective_id=1, has_side_effects=True, vmem_limit_bytes=grant(ep_count)
         ),
         name="spread",
     )(partial, stream, gain, meta)
@@ -339,13 +410,14 @@
             dma((more, side, line)), dma((more, line)), dma((max(line - 1, 1),)),
         ],
         compiler_params=pltpu.CompilerParams(
-            collective_id=2, has_side_effects=True, vmem_limit_bytes=VMEM_SMALL
+            collective_id=2, has_side_effects=True, vmem_limit_bytes=grant(ep_count)
         ),
         name="collect",
     )(own.reshape((ep_count,) + block), theirs.reshape((ep_count,) + block), kept)
 
 
-VMEM_SMALL = 40 * 1024 * 1024
+def grant(ep_count):
+    return max(8, ep_count // 2) * 1024 * 1024
 
 
 def local(

time: 120 us -> 101 us (0.84)
  other arithmetic: 19.3 us -> 4.07 us
  local copies, waits for them, and re-layouts: 20.3 us -> 10.8 us
  Pallas kernels: 44.7 us -> 50.5 us
    mul x1 -> x0, other arithmetic: 8.62 us -> none  [mix_heads(): (step_size[:, :, None] * values)[:, :, :, None] * write_map[:, :, None, :]]
    mul x1, local copies, waits for them, and re-layouts: 7.88 us -> 0.09 us  [mix_heads(): step_size[:, :, None] * values]
    reshape x1, local copies, waits for them, and re-layouts: 7.88 us -> 0.09 us  [mix_heads(): read.reshape(row_count, head_count, HEAD) + skip_gain[:, None] * values]
    add x1 -> x0, other arithmetic: 6.58 us -> none  [mix_heads(): decay_now[:, :, None, None] * state_old]
    pallas_call x0 -> x1, Pallas kernels: none -> 5.79 us  [step_state(): pl.pallas_call(state_kernel, grid=(flat // rows,), out_shape=(jax.ShapeDt...]
    unnamed x59 -> x65, local copies, waits for them, and re-layouts: 1.8 us -> 6.22 us
    slice x1, local copies, waits for them, and re-layouts: 0.19 us -> 1.73 us  [local(): all_own = every[0].reshape(total_rows, half)]
  transfers between devices with their start and end apart: 3 -> 3, of which waited for: 0 -> 0; matrix products, arithmetic and copies ran while one was open for 58% -> 40% of each run, Pallas kernels for 20% -> 29%
where the time goes in v2:
time: 101 us; the launch traced here: 100 us
  Pallas kernels  50.5 us (50%)
  matrix products  32.4 us (32%)
  local copies, waits for them, and re-layouts  10.8 us (11%)
  other arithmetic  4.07 us (4%)
  between operations  1.28 us (1%)
  starting transfers between devices  1.13 us (1%)
    pallas_call x1, Pallas kernels, spread(): pl.pallas_call(functools.partial(spread_kernel, ep_count), out_shape=(jax...  23.2 us
    pallas_call x1, Pallas kernels, collect(): pl.pallas_call(functools.partial(collect_kernel, ep_count), out_shape=jax...  21.5 us
    dot_general x8, matrix products, f32_dot(): return jnp.dot(left, right, preferred_element_type=jnp.float32)  21.1 us
    unnamed x65, local copies, waits for them, and re-layouts  6.22 us
    pallas_call x1, Pallas kernels, step_state(): pl.pallas_call(state_kernel, grid=(flat // rows,), out_shape=(jax.ShapeDt...  5.79 us
    dot_general x2, matrix products, result(): lax.dot_general(pick, share_half, (((0,), (0,)), ((), ())), preferred_ele...  3.53 us
    select_n x2, other arithmetic, mine(): return jnp.where(first, left, right)  3.08 us
    dot_general x1, matrix products, mix_heads(): jnp.dot(normed, gate_proj, preferred_element_type=jnp.float32)  2.13 us
  transfers between devices with their start and end apart: 3, of which 0 were waited for; matrix products, arithmetic and copies ran while one was open for 40% of the time, Pallas kernels for 29%

profile of v2, /device:TPU:0, one launch (start us, length us, event | category | flops | bytes accessed | tf_op | source)
XLA Modules:
  0.0 100.2 jit_solution(3819821595114738175)
XLA Ops:
  0.6 0.6 collective-permute-start.2
  1.2 1.9 %broadcast_select_fusion.3 = bf16[176,1024]{1,0:T(8,128)(2,1)} fusion(pred[]{:T(512)S(6)} %eq.56, bf16[352,1024]{1,0:T(8,128)(2,1)} %param.50), kind=kLoop, calls=%fused_computation.45 | loop fusion | flops 180224 | bytes 1081345 | tf_op jit(solution)/shard_map/jit(_where)/select_n | solution.py:457
  3.2 1.4 %fusion.58 = (bf16[1024,176]{0,1:T(8,128)(2,1)S(1)}, bf16[1024,176]{0,1:T(8,128)(2,1)S(1)}, bf16[1024,176]{0,1:T(8,128)(2,1)S(1)}, bf16[1024,176]{0,1:T(8,128)(2,1)S(1)}) fusion(bf16[1024,352]{0,1:T(8,128)(2,1)} %param.48, bf16[1024,352]{0,1:T(8,128)(2,1)} %param.49), kind=kLoop, calls=%fused_computation.108 | loop fusion | bytes 2883584 | tf_op jit(solution)/shard_map/slice | solution.py:459
  4.8 0.6 copy-done.6
  5.4 1.1 %broadcast_select_fusion = bf16[1024,352]{0,1:T(8,128)(2,1)} fusion(pred[]{:T(512)S(6)} %eq.56, bf16[1024,176]{0,1:T(8,128)(2,1)S(1)} %get-tuple-element.30, bf16[1024,176]{0,1:T(8,128)(2,1)S(1)} %get-tuple-element.19, bf16[1024,176]{0,1:T(8,128)(2,1)S(1)} %get-tuple-element.31, bf16[1024,176]{0,1:T(8,128)(2,1)S(1)} %get-tuple-element.18), kind=kLoop, calls=%fused_computation.25 | loop fusion | flops 3244032 | bytes 2162689 | tf_op jit(solution)/shard_map/jit(_where)/select_n | solution.py:457
  6.5 0.5 collective-permute-start
  7.2 1.3 %fusion.4 = bf16[32,1,1,128]{3,0,2,1:T(8,128)(2,1)S(1)} fusion(bf16[2,2048,128]{2,1,0:T(8,128)(2,1)} %param.30, bf16[32,2048]{1,0:T(8,128)(2,1)S(1)} %copy-done.2, f32[2048]{0:T(1024)S(1)} %copy-done.18, f32[32]{0:T(128)S(1)} %add_rsqrt_fusion.1), kind=kOutput, calls=%fused_computation.16 | convolution fusion | flops 17043456 | bytes 671872 | tf_op jit(solution)/shard_map/dot_general | solution.py:118
  8.5 1.3 %fusion.5 = bf16[32,1,1,128]{3,0,2,1:T(8,128)(2,1)S(1)} fusion(bf16[2,2048,128]{2,1,0:T(8,128)(2,1)} %param.30, bf16[32,2048]{1,0:T(8,128)(2,1)S(1)} %copy-done.2, f32[2048]{0:T(1024)S(1)} %copy-done.18, f32[32]{0:T(128)S(1)} %add_rsqrt_fusion.1), kind=kOutput, calls=%fused_computation.17 | convolution fusion | flops 17043456 | bytes 671872 | tf_op jit(solution)/shard_map/dot_general | solution.py:119
  10.4 0.2 multiply_exponential_fusion
  11.2 2.1 %fusion.3 = bf16[32,1,512]{2,0,1:T(8,128)(2,1)S(1)} fusion(bf16[2048,512]{1,0:T(8,128)(2,1)} %param.29, bf16[32,2048]{1,0:T(8,128)(2,1)S(1)} %copy-done.2, f32[2048]{0:T(1024)S(1)} %copy-done.18, f32[32]{0:T(128)S(1)} %add_rsqrt_fusion.1), kind=kOutput, calls=%fused_computation.13 | convolution fusion | flops 67387392 | bytes 2269312 | tf_op jit(solution)/shard_map/dot_general | solution.py:115
  13.7 2.2 %copy-done.1 = f32[32,8,4096]{2,1,0:T(8,128)S(1)} copy-done((f32[32,8,4096]{2,1,0:T(8,128)S(1)}, f32[32,8,4096]{2,1,0:T(8,128)}, u32[]{:S(2)}) %copy-start.1) | copy-done | bytes 4194328
  15.9 5.8 %state.1 = (f32[256,4096]{1,0:T(8,128)}, f32[256,64]{1,0:T(8,128)S(1)}) custom-call(f32[256,4096]{1,0:T(8,128)S(1)} %bitcast.44, f32[256,64]{1,0:T(8,128)S(1)} %multiply_multiply_fusion.fed, f32[256,64]{1,0:T(8,128)S(1)} %bitcast.46, f32[256,64]{1,0:T(8,128)S(1)} %bitcast.47, f32[256,128]{1,0:T(8,128)S(1)} %broadcast_in_dim.89.decay), custom_call_target="tpu_custom_call" | custom-call | tf_op jit(solution)/shard_map/state/pallas_call | solution.py:78
  21.8 2.1 %fusion.61 = (f32[32,512]{1,0:T(8,128)S(1)}, f32[32,512]{1,0:T(8,128)S(1)}) fusion(bf16[2048,512]{1,0:T(8,128)(2,1)} %param.28, bf16[32,2048]{1,0:T(8,128)(2,1)S(1)} %copy-done.2, f32[2048]{0:T(1024)S(1)} %copy-done.18, f32[32]{0:T(128)S(1)} %add_rsqrt_fusion.1, f32[32,512]{1,0:T(8,128)S(1)} %reshape.187, f32[32,512]{1,0:T(8,128)S(1)} %multiply_reduce_fusion, ...), kind=kOutput, calls=%fused_computation.111 | convolution fusion | flops 67600384 | bytes 2500736 | tf_op jit(solution)/shard_map/dot_general | solution.py:114
  24.5 0.5 convolution_convert_fusion.partial
  25.0 23.2 %spread.1 = (bf16[2,16,32,1024]{3,2,1,0:T(8,128)(2,1)S(1)}, f32[16,8,128]{2,1,0:T(8,128)S(1)}, f32[32,1024]{1,0:T(8,128)S(1)}) custom-call(bf16[32,2048]{1,0:T(8,128)(2,1)S(1)} %convolution_convert_fusion.partial, bf16[32,2048]{1,0:T(8,128)(2,1)S(1)} %copy-done.2, f32[1,2048]{1,0:T(1,128)S(1)} %bitcast.48, f32[8,128]{1,0:T(8,128)S(1)} %select_maximum_fusion.meta), custom_call_target="tpu_custom_call" | custom-call | tf_op jit(solution)/shard_map/spread/pallas_call | solution.py:303
  48.2 1.3 %copy-done.3 = bf16[2,16,32,1024]{3,2,1,0:T(8,128)(2,1)} copy-done((bf16[2,16,32,1024]{3,2,1,0:T(8,128)(2,1)}, bf16[2,16,32,1024]{3,2,1,0:T(8,128)(2,1)S(1)}, u32[]{:S(2)}) %copy-start.3) | copy-done | bytes 2097176
  49.8 1.7 %fusion.57 = (bf16[1,16,32,1024]{3,2,1,0:T(8,128)(2,1)S(1)}, bf16[1,16,32,1024]{3,2,1,0:T(8,128)(2,1)S(1)}) fusion(bf16[2,16,32,1024]{3,2,1,0:T(8,128)(2,1)} %copy-done.3), kind=kLoop, calls=%fused_computation.107 | loop fusion | bytes 4194304 | tf_op jit(solution)/shard_map/slice | solution.py:503
  51.6 0.2 select_reduce_fusion
  51.8 0.4 convolution_convert_fusion.1
  52.2 0.3 copy-done.14
  52.5 0.4 broadcast_select_fusion.2
  53.0 0.7 copy-done.29
  53.9 5.8 %fusion.13 = f32[192,1792]{1,0:T(8,128)} fusion(bf16[2048,1792]{1,0:T(8,128)(2,1)} %param.45, bf16[192,1024]{1,0:T(8,128)(2,1)S(1)} %get-tuple-element.17, bf16[192,1024]{1,0:T(8,128)(2,1)S(1)} %get-tuple-element.16), kind=kOutput, calls=%fused_computation.31 | convolution fusion | flops 1410859008 | bytes 9502720 | tf_op jit(solution)/shard_map/dot_general | solution.py:507
  59.7 10.2 %fusion = bf16[192,2048]{1,0:T(8,128)(2,1)} fusion(bf16[1792,2048]{1,0:T(8,128)(2,1)} %param.47, f32[192]{0:T(256)S(1)} %select_reduce_fusion, bf16[2048,1792]{1,0:T(8,128)(2,1)} %param.46, f32[192,1792]{1,0:T(8,128)} %fusion.13, bf16[192,1024]{1,0:T(8,128)(2,1)} %copy-done.30, bf16[192,1024]{1,0:T(8,128)(2,1)} %copy-done.29), kind=kOutput, calls=%fused_computation.2 | convolution fusion | flops 2822995968 | bytes 17629952 | tf_op jit(solution)/shard_map/dot_general | solution.py:507
  69.9 1.8 %fusion.16 = f32[512,1024]{1,0:T(8,128)S(1)} fusion(pred[]{:T(512)S(6)} %eq.56, bf16[192,2048]{1,0:T(8,128)(2,1)} %fusion, f32[512]{0:T(512)S(1)} %eq.53, s32[512]{0:T(512)S(1)} %add_select_fusion, f32[192]{0:T(256)S(1)} %get-tuple-element.29, s32[192]{0:T(256)S(1)} %get-tuple-element.28), kind=kOutput, calls=%fused_computation.34 | convolution fusion | flops 201818112 | bytes 2889217 | tf_op jit(solution)/shard_map/dot_general | solution.py:521
  71.8 1.7 %fusion.14 = f32[512,1024]{1,0:T(8,128)S(1)} fusion(pred[]{:T(512)S(6)} %eq.56, bf16[192,2048]{1,0:T(8,128)(2,1)} %fusion, f32[512]{0:T(512)S(1)} %eq.53, s32[512]{0:T(512)S(1)} %add_select_fusion, f32[192]{0:T(256)S(1)} %get-tuple-element.29, s32[192]{0:T(256)S(1)} %get-tuple-element.28), kind=kOutput, calls=%fused_computation.32 | convolution fusion | flops 201818112 | bytes 2889217 | tf_op jit(solution)/shard_map/dot_general | solution.py:521
  73.5 0.6 fusion.6
  74.3 1.7 %convolution_add_fusion = f32[512,352]{0,1:T(8,128)S(1)} fusion(f32[512,352]{0,1:T(8,128)S(1)} %fusion.6, bf16[512,1024]{1,0:T(8,128)(2,1)S(1)} %bitcast.50, bf16[1024,352]{0,1:T(8,128)(2,1)} %collective-permute-done), kind=kOutput, calls=%fused_computation.7 | convolution fusion | flops 369278976 | bytes 3211264 | tf_op jit(solution)/shard_map/dot_general | solution.py:507
  76.1 0.5 add_convert_fusion.1
  76.6 1.5 %add_convert_fusion = bf16[512,1024]{1,0:T(8,128)(2,1)S(1)} fusion(f32[512,1024]{1,0:T(8,128)S(1)} %fusion.14, bf16[512,176]{0,1:T(8,128)(2,1)S(1)} %fusion.20, bf16[176,1024]{1,0:T(8,128)(2,1)} %collective-permute-done.1, f32[1024]{0:T(1024)S(1)} %add_divide_fusion), kind=kOutput, calls=%fused_computation.5 | convolution fusion | flops 186122240 | bytes 3690496 | tf_op jit(solution)/shard_map/dot_general | solution.py:507
  78.1 21.5 %collect.1 = bf16[32,1024]{1,0:T(8,128)(2,1)S(1)} custom-call(bf16[16,32,1024]{2,1,0:T(8,128)(2,1)S(1)} %bitcast.43, bf16[16,32,1024]{2,1,0:T(8,128)(2,1)S(1)} %bitcast.45, f32[32,1024]{1,0:T(8,128)S(1)} %get-tuple-element.10.kept), custom_call_target="tpu_custom_call" | custom-call | tf_op jit(solution)/shard_map/collect/pallas_call | solution.py:398
  99.6 0.6 copy.50
  (104 shorter events, 2.9 us)
Async XLA Ops:
  0.6 23.9 %copy-start = (bf16[512,2048]{1,0:T(8,128)(2,1)S(1)}, bf16[512,2048]{1,0:T(8,128)(2,1)}, u32[]{:S(2)}) copy-start(bf16[512,2048]{1,0:T(8,128)(2,1)} %param.41) | copy-start | bytes 6291460
  0.6 73.6 %collective-permute-start.2 = (f32[1024]{0:T(1024)}, f32[1024]{0:T(1024)S(1)}, u32[]{:S(2)}, u32[]{:S(2)}) collective-permute-start(f32[1024]{0:T(1024)} %param.51), channel_id=1, source_target_pairs={{0,1},{1,0},{2,3},{3,2},{4,5},{5,4},{6,7},{7,6},{8,9},{9,8},{10,11... | collective-permute-start | bytes 12296 | tf_op jit(solution)/shard_map/ppermute | solution.py:465
  3.1 3.9 %copy-start.2 = (bf16[32,2048]{1,0:T(8,128)(2,1)S(1)}, bf16[32,2048]{1,0:T(8,128)(2,1)}, u32[]{:S(2)}) copy-start(bf16[32,2048]{1,0:T(8,128)(2,1)} %stream.1) | copy-start | bytes 393220
  3.1 4.0 %copy-start.18 = (f32[2048]{0:T(1024)S(1)}, f32[2048]{0:T(1024)}, u32[]{:S(2)}) copy-start(f32[2048]{0:T(1024)} %param.27) | copy-start | bytes 24580
  3.2 73.5 %collective-permute-start.1 = (bf16[176,1024]{1,0:T(8,128)(2,1)}, bf16[176,1024]{1,0:T(8,128)(2,1)}, u32[]{:S(2)}, u32[]{:S(2)}) collective-permute-start(bf16[176,1024]{1,0:T(8,128)(2,1)} %broadcast_select_fusion.3), channel_id=1, source_target_pairs={{0,1},{1,0},{2,3},{3,2},{4,5},{5,4},{6,7},{7,6},{8,9},{9,8},{10,11... | collective-permute-start | bytes 1081352 | tf_op jit(solution)/shard_map/ppermute | solution.py:464
  4.7 1.9 %copy-start.8 = (bf16[1024,176]{0,1:T(8,128)(2,1)}, bf16[1024,176]{0,1:T(8,128)(2,1)S(1)}, u32[]{:S(2)}) copy-start(bf16[1024,176]{0,1:T(8,128)(2,1)S(1)} %get-tuple-element.19) | copy-start | bytes 1081348
  4.7 1.9 %copy-start.10 = (bf16[1024,176]{0,1:T(8,128)(2,1)}, bf16[1024,176]{0,1:T(8,128)(2,1)S(1)}, u32[]{:S(2)}) copy-start(bf16[1024,176]{0,1:T(8,128)(2,1)S(1)} %get-tuple-element.30) | copy-start | bytes 1081348
  4.7 1.8 %copy-start.12 = (bf16[1024,176]{0,1:T(8,128)(2,1)}, bf16[1024,176]{0,1:T(8,128)(2,1)S(1)}, u32[]{:S(2)}) copy-start(bf16[1024,176]{0,1:T(8,128)(2,1)S(1)} %get-tuple-element.31) | copy-start | bytes 1081348
  4.7 5.2 %copy-start.27 = (f32[8]{0:T(128)S(1)}, f32[8]{0:T(128)}, u32[]{:S(2)}) copy-start(f32[8]{0:T(128)} %param.33) | copy-start | bytes 100
  4.7 5.2 %copy-start.22 = (s32[32,2]{0,1:T(2,128)S(1)}, s32[32,2]{0,1:T(2,128)}, u32[]{:S(2)}) copy-start(s32[32,2]{0,1:T(2,128)} %param.43) | copy-start | bytes 772
  4.7 5.2 %copy-start.20 = (f32[2,4,128]{2,1,0:T(4,128)S(1)}, f32[2,4,128]{2,1,0:T(4,128)}, u32[]{:S(2)}) copy-start(f32[2,4,128]{2,1,0:T(4,128)} %param.35) | copy-start | bytes 12292
  4.7 5.2 %copy-start.25 = (f32[8]{0:T(128)S(1)}, f32[8]{0:T(128)}, u32[]{:S(2)}) copy-start(f32[8]{0:T(128)} %param.39) | copy-start | bytes 100
  4.8 5.4 %copy-start.24 = (f32[32,2]{0,1:T(2,128)S(1)}, f32[32,2]{0,1:T(2,128)}, u32[]{:S(2)}) copy-start(f32[32,2]{0,1:T(2,128)} %param.44) | copy-start | bytes 772
  4.8 5.4 %copy-start.17 = (bf16[32,2,3,128]{3,1,2,0:T(2,128)(2,1)S(1)}, bf16[32,2,3,128]{3,1,2,0:T(2,128)(2,1)}, u32[]{:S(2)}) copy-start(bf16[32,2,3,128]{3,1,2,0:T(2,128)(2,1)} %param.37) | copy-start | bytes 147460
  5.4 5.0 %copy-start.26 = (bf16[2048,8]{0,1:T(8,128)(2,1)S(1)}, bf16[2048,8]{0,1:T(8,128)(2,1)}, u32[]{:S(2)}) copy-start(bf16[2048,8]{0,1:T(8,128)(2,1)} %param.31) | copy-start | bytes 98308
  5.4 5.0 %copy-start.28 = (f32[8]{0:T(128)S(1)}, f32[8]{0:T(128)}, u32[]{:S(2)}) copy-start(f32[8]{0:T(128)} %param.32) | copy-start | bytes 100
  6.5 67.7 %collective-permute-start = (bf16[1024,352]{0,1:T(8,128)(2,1)}, bf16[1024,352]{0,1:T(8,128)(2,1)}, u32[]{:S(2)}, u32[]{:S(2)}) collective-permute-start(bf16[1024,352]{0,1:T(8,128)(2,1)} %broadcast_select_fusion), channel_id=1, source_target_pairs={{0,1},{1,0},{2,3},{3,2},{4,5},{5,4},{6,7},{7,6},{8,9},{9,8},{10,11... | collective-permute-start | bytes 2162696 | tf_op jit(solution)/shard_map/ppermute | solution.py:462
  8.5 4.8 %copy-start.16 = (bf16[32,3,512]{2,0,1:T(8,128)(2,1)S(1)}, bf16[32,3,512]{2,0,1:T(8,128)(2,1)}, u32[]{:S(2)}) copy-start(bf16[32,3,512]{2,0,1:T(8,128)(2,1)} %param.36) | copy-start | bytes 294916
  8.5 4.8 %copy-start.19 = (f32[4,512]{1,0:T(4,128)S(1)}, f32[4,512]{1,0:T(4,128)}, u32[]{:S(2)}) copy-start(f32[4,512]{1,0:T(4,128)} %param.34) | copy-start | bytes 24580
  13.7 2.2 %copy-start.1 = (f32[32,8,4096]{2,1,0:T(8,128)S(1)}, f32[32,8,4096]{2,1,0:T(8,128)}, u32[]{:S(2)}) copy-start(f32[32,8,4096]{2,1,0:T(8,128)} %param.38) | copy-start | bytes 12582916
  21.7 2.8 %copy-start.23 = (f32[512]{0:T(512)S(1)}, f32[512]{0:T(512)}, u32[]{:S(2)}) copy-start(f32[512]{0:T(512)} %param.40) | copy-start | bytes 6148
  21.8 3.2 %copy-start.4 = (f32[2048]{0:T(1024)S(1)}, f32[2048]{0:T(1024)}, u32[]{:S(2)}) copy-start(f32[2048]{0:T(1024)} %param.42) | copy-start | bytes 24580
  48.2 1.3 %copy-start.3 = (bf16[2,16,32,1024]{3,2,1,0:T(8,128)(2,1)}, bf16[2,16,32,1024]{3,2,1,0:T(8,128)(2,1)S(1)}, u32[]{:S(2)}) copy-start(bf16[2,16,32,1024]{3,2,1,0:T(8,128)(2,1)S(1)} %get-tuple-element.9) | copy-start | bytes 6291460
  51.6 1.0 copy-start.14
  53.0 0.8 copy-start.29
  53.0 0.9 copy-start.30
  69.9 3.6 %copy-start.7 = (bf16[1024,176]{0,1:T(8,128)(2,1)S(1)}, bf16[1024,176]{0,1:T(8,128)(2,1)}, u32[]{:S(2)}) copy-start(bf16[1024,176]{0,1:T(8,128)(2,1)} %copy-done.6) | copy-start | bytes 1081348
  69.9 3.6 %copy-start.9 = (bf16[1024,176]{0,1:T(8,128)(2,1)S(1)}, bf16[1024,176]{0,1:T(8,128)(2,1)}, u32[]{:S(2)}) copy-start(bf16[1024,176]{0,1:T(8,128)(2,1)} %copy-done.8) | copy-start | bytes 1081348
  69.9 3.6 %copy-start.11 = (bf16[1024,176]{0,1:T(8,128)(2,1)S(1)}, bf16[1024,176]{0,1:T(8,128)(2,1)}, u32[]{:S(2)}) copy-start(bf16[1024,176]{0,1:T(8,128)(2,1)} %copy-done.10) | copy-start | bytes 1081348
  69.9 3.6 %copy-start.13 = (bf16[1024,176]{0,1:T(8,128)(2,1)S(1)}, bf16[1024,176]{0,1:T(8,128)(2,1)}, u32[]{:S(2)}) copy-start(bf16[1024,176]{0,1:T(8,128)(2,1)} %copy-done.12) | copy-start | bytes 1081348
  69.9 3.6 %copy-start.15 = (bf16[1,16,32,1024]{3,2,1,0:T(8,128)(2,1)S(1)}, bf16[1,16,32,1024]{3,2,1,0:T(8,128)(2,1)}, u32[]{:S(2)}) copy-start(bf16[1,16,32,1024]{3,2,1,0:T(8,128)(2,1)} %copy-done.14) | copy-start | bytes 3145732
  74.2 1.9 %copy-start.5 = (bf16[352,1024]{1,0:T(8,128)(2,1)S(1)}, bf16[352,1024]{1,0:T(8,128)(2,1)}, u32[]{:S(2)}) copy-start(bf16[352,1024]{1,0:T(8,128)(2,1)} %param.50) | copy-start | bytes 2162692
  (2 other events, 1.4 us)
